TPU v7x, 32 devices: a whole 2x2x4 slice. The times are simulated.
32 devices in a mesh: gr: 2 (over core), sp: 8 (over z, y), tp: 2 (over x).
Axes of the slice: x: 2, y: 2, z: 4, core: 2. Of those that a mesh axis runs over, the one named last changes fastest.
Arguments:
- tokens: bfloat16 [4, 2048, 2048], P('gr', ('sp', 'tp')), parts along dimension 0, may hold values from -6 to 6
- key_weight: bfloat16 [2048, 1024], P('sp'), may hold values from -0.125 to 0.125
- value_weight: bfloat16 [2048, 1024], P('sp'), may hold values from -0.125 to 0.125
- queries: bfloat16 [4, 1024], P('gr'), parts along dimension 0, may hold values from -6 to 6
- head_offset: float32 [16], replicated, may hold values from -14 to -3.5
- key_bias: bfloat16 [4, 2048, 16], P('gr', ('sp', 'tp')), parts along dimension 0, may hold values from -0.5 to 12.9
Outputs:
- key_cache: bfloat16 [4, 2048, 1024], P('gr', 'sp', 'tp'), parts along dimension 0
- value_cache: bfloat16 [4, 2048, 1024], P('gr', 'sp', 'tp'), parts along dimension 0
- bias_cache: bfloat16 [4, 2048, 16], P('gr', 'sp', 'tp'), parts along dimension 0
- reading: float32 [4, 1024], P('gr', 'tp'), parts along dimension 0
There are 2 independent parts, one for each index of `gr`. A program takes and returns all parts, laid end to end along the dimension named above; an argument that names none is the same for every part. Nothing has to cross between parts.
All inputs are finite; a program needn't handle non-finite values.
Results may differ from a plain program's by a relative error of at most 0.0052.
Values may be sent and summed in bfloat16 or wider, within the bound.
No kernel may reach another device: no remote copies, remote signals or barrier semaphores. Data moves between devices by JAX's collectives and lax.ppermute only.
A program may use at most 64 MiB of HBM per device.

v0:
```python
import jax
import jax.numpy as jnp
from jax import lax
from jax.sharding import PartitionSpec as P


def carried_in(x, axis, combine, identity):
    length, position = (lax.axis_size(axis), lax.axis_index(axis))
    everything = lax.all_gather(x, axis)
    start = jnp.broadcast_to(jnp.asarray(identity, x.dtype), x.shape)

    def lap(k, before):
        at = length - 1 - k
        reached = at > position
        new = combine(before, everything[at])
        return jnp.where(reached, new, before)

    return lax.fori_loop(0, length, lap, start)


def add_terms(earlier, later):
    return earlier + later


def normalize(mixture):
    return mixture * lax.rsqrt(jnp.mean(mixture * mixture, axis=-1, keepdims=True) + 1e-06)


def per_device(tokens, key_weight, value_weight, queries, head_offset, key_bias):
    seq_count, pos_dev, model_width = tokens.shape
    head_count = head_offset.shape[0]
    kv_width = key_weight.shape[1]
    head_dim = kv_width // head_count
    score_scale = head_dim ** (-0.5)
    tp_count = lax.axis_size("tp")
    col_width = kv_width // tp_count
    col_start = lax.axis_index("tp") * col_width
    own_cols = jnp.concatenate(
        [
            lax.dynamic_slice_in_dim(key_weight, col_start, col_width, 1),
            lax.dynamic_slice_in_dim(value_weight, col_start, col_width, 1),
        ],
        axis=1,
    )
    full_cols = lax.all_gather(own_cols, "sp", axis=0, tiled=True)
    projected = jnp.einsum(
        "spd,dw->spw",
        lax.all_gather(tokens, "tp", axis=1, tiled=True),
        full_cols,
        preferred_element_type=jnp.float32,
    ).astype(jnp.bfloat16)
    key_cache = projected[:, :, :col_width]
    value_cache = projected[:, :, col_width:]
    bias_cache = lax.all_to_all(key_bias, "tp", split_axis=2, concat_axis=1, tiled=True)
    span_len = key_cache.shape[1]
    local_heads = bias_cache.shape[2]
    key_blocks = key_cache.reshape(seq_count, span_len, local_heads, head_dim)
    value_blocks = value_cache.reshape(seq_count, span_len, local_heads, head_dim)
    query_cols = lax.dynamic_slice_in_dim(queries, col_start, col_width, 1)
    query_heads = query_cols.reshape(seq_count, local_heads, head_dim)
    head_start = lax.axis_index("tp") * local_heads
    local_offset = lax.dynamic_slice_in_dim(head_offset, head_start, local_heads, 0)
    logits = (
        jnp.einsum("sphc,shc->shp", key_blocks, query_heads, preferred_element_type=jnp.float32)
        * score_scale
    )
    logits = (
        logits
        + local_offset[None, :, None]
        + jnp.transpose(bias_cache.astype(jnp.float32), (0, 2, 1))
    )
    fading = jax.nn.log_sigmoid(-logits)
    within = lax.cumsum(fading, axis=2, reverse=True) - fading
    block_total = jnp.sum(fading, axis=2)
    carried = carried_in(block_total, "sp", add_terms, jnp.zeros_like(block_total))
    weights = jnp.exp(jax.nn.log_sigmoid(logits) + within + carried[:, :, None]).astype(
        jnp.bfloat16
    )
    partial_value = jnp.einsum(
        "shp,sphc->shc", weights, value_blocks, preferred_element_type=jnp.float32
    )
    mixture = lax.psum(partial_value, "sp")
    reading = normalize(mixture).reshape(seq_count, col_width)
    return (key_cache, value_cache, bias_cache, reading)


def solution(mesh):
    in_specs = (
        P("gr", ("sp", "tp"), None),
        P("sp", None),
        P("sp", None),
        P("gr", None),
        P(),
        P("gr", ("sp", "tp"), None),
    )
    out_specs = (P("gr", "sp", "tp"), P("gr", "sp", "tp"), P("gr", "sp", "tp"), P("gr", "tp"))
    return jax.shard_map(
        per_device, mesh=mesh, in_specs=in_specs, out_specs=out_specs, check_vma=False
    )
```

profile of v0, /device:TPU:0, one launch (start us, length us, event | category | flops | bytes accessed | tf_op | source)
XLA Modules:
  0.0 179.6 jit_solution(294673093222609058)
XLA Ops:
  7.2 0.7 all-gather.7.cloned.1.call-update
  8.0 1.1 constant_dynamic-slice_fusion.1
  9.1 0.1 copy.28
  9.2 0.1 copy.29
  9.3 0.8 pad_maximum_fusion
  10.2 0.6 copy.20
  10.8 4.2 %all-to-all-start = ((bf16[2,128,16]{1,0,2:T(2,128)(2,1)}), bf16[2,128,16]{1,0,2:T(2,128)(2,1)S(1)}, u32[]{:S(2)}, u32[]{:S(2)}) async-start(bf16[2,128,16]{1,0,2:T(2,128)(2,1)} %copy.20), calls=%async_computation | async-start | bytes 16384 | tf_op jit(solution)/shard_map/all_to_all | solution.py:54
  15.2 30.2 %all-gather.7.cloned.1.call-done = bf16[2,256,2048]{2,1,0:T(8,128)(2,1)} async-done(((bf16[2,128,2048]{2,1,0:T(8,128)(2,1)}), bf16[2,256,2048]{2,1,0:T(8,128)(2,1)}) %all-gather.7.cloned.1.call-update) | async-done | bytes 2097168 | tf_op jit(solution)/shard_map/all_gather | solution.py:48
  45.4 77.3 %all-gather.5.cloned.1.call-done = bf16[2048,1024]{0,1:T(8,128)(2,1)} async-done(((bf16[256,1024]{0,1:T(8,128)(2,1)}), bf16[2048,1024]{0,1:T(8,128)(2,1)}) %all-gather.5.cloned.1.call-update) | async-done | bytes 4194320 | tf_op jit(solution)/shard_map/all_gather | solution.py:45
  122.7 5.2 %fusion.5 = bf16[2,256,1024]{1,2,0:T(8,128)(2,1)S(1)} fusion(bf16[2,256,2048]{2,1,0:T(8,128)(2,1)} %all-gather.7.cloned.1.call-done, bf16[2048,1024]{0,1:T(8,128)(2,1)} %all-gather.5.cloned.1.call-done), kind=kOutput, calls=%fused_computation.4 | convolution fusion | flops 2148007936 | bytes 7340032 | tf_op jit(solution)/shard_map/spd,dw->spw/dot_general | solution.py:46
  128.0 0.2 fusion.19
  128.2 1.0 copy.22
  129.2 0.1 negate_bitcast_fusion
  129.3 0.2 fusion.16
  129.5 17.7 %all-gather.1 = f32[8,2,8]{2,1,0:T(2,128)S(1)} all-gather(f32[1,2,8]{2,1,0:T(2,128)S(1)} %negate_bitcast_fusion.1), channel_id=2, replica_groups=mesh['gr'=2,'sp'=8,'tp'=2] {'sp'}, dimensions={0}, use_global_device_ids=true | all-gather | bytes 576 | tf_op jit(solution)/shard_map/all_gather | solution.py:9
  147.2 0.3 while.16
  147.5 5.0 %reduce-window.6 = f32[2,8,2,128]{3,1,2,0:T(8,128)S(1)} reduce-window(f32[2,8,2,128]{3,1,2,0:T(8,128)S(1)} %get-tuple-element.150, f32[]{:T(128)} %constant.72.clone.1), window={size=1x1x1x128 pad=0_0x0_0x0_0x0_127}, to_apply=%region_0.1 | reduce-window | flops 520192 | bytes 32772 | tf_op jit(solution)/shard_map/reduce-window
  152.5 0.1 slice_reduce_fusion
  152.6 1.0 copy.23
  153.6 0.1 fusion.17
  153.7 0.2 fusion.14
  153.9 17.9 %psum.7 = f32[2,8,64]{2,1,0:T(8,128)S(1)} all-reduce(f32[2,8,64]{2,1,0:T(8,128)S(1)} %bitcast.62), channel_id=1, replica_groups=mesh['gr'=2,'sp'=8,'tp'=2] {'sp'}, use_global_device_ids=true, to_apply=%region_5.6 | all-reduce | flops 1024 | bytes 8192 | tf_op jit(solution)/shard_map/psum | solution.py:82
  171.9 0.1 multiply_reduce_fusion
  172.1 0.7 reshape.53
  (30 shorter events, 0.6 us)
Async XLA Ops:
  7.2 7.9 %copy-start = (bf16[2,1024]{1,0:T(2,128)(2,1)S(1)}, bf16[2,1024]{1,0:T(2,128)(2,1)}, u32[]{:S(2)}) copy-start(bf16[2,1024]{1,0:T(2,128)(2,1)} %param.11) | copy-start | bytes 12292
  7.2 38.2 %all-gather.7.cloned.1.call-start = ((), (), s32[]{:S(2)}) async-start(), calls=%async_computation.2 | async-start | bytes 3145728 | tf_op jit(solution)/shard_map/all_gather | solution.py:48
  7.9 2.3 %copy-start.2 = (bf16[2,128,16]{1,2,0:T(8,128)(2,1)S(1)}, bf16[2,128,16]{1,2,0:T(8,128)(2,1)}, u32[]{:S(2)}) copy-start(bf16[2,128,16]{1,2,0:T(8,128)(2,1)} %param.13) | copy-start | bytes 24580
  7.9 7.2 %copy-start.3 = (f32[16]{0:T(128)S(1)}, f32[16]{0:T(128)}, u32[]{:S(2)}) copy-start(f32[16]{0:T(128)} %param.12) | copy-start | bytes 196
  7.9 114.7 %all-gather.5.cloned.1.call-start = ((), (), s32[]{:S(2)}) async-start(), calls=%async_computation.1 | async-start | bytes 4718592 | tf_op jit(solution)/shard_map/all_gather | solution.py:45
  10.8 118.4 %all-to-all-start = ((bf16[2,128,16]{1,0,2:T(2,128)(2,1)}), bf16[2,128,16]{1,0,2:T(2,128)(2,1)S(1)}, u32[]{:S(2)}, u32[]{:S(2)}) async-start(bf16[2,128,16]{1,0,2:T(2,128)(2,1)} %copy.20), calls=%async_computation | async-start | bytes 16384 | tf_op jit(solution)/shard_map/all_to_all | solution.py:54
  129.3 43.5 %copy-start.1 = (bf16[2,256,8]{1,2,0:T(8,128)(2,1)}, bf16[2,256,8]{1,2,0:T(8,128)(2,1)S(1)}, u32[]{:S(2)}) copy-start(bf16[2,256,8]{1,2,0:T(8,128)(2,1)S(1)} %get-tuple-element.151) | copy-start | bytes 24580
Sparse Core Ops, SparseCore 0:
  9.5 35.8 all-gather.6
  48.0 74.6 all-gather.4
where the time goes:
time: 180 us
  waiting for transfers between devices  108 us (60%)
  blocking collectives  35.7 us (20%)
  between operations  14.2 us (8%)
  other arithmetic  6.49 us (4%)
  matrix products  5.64 us (3%)
  local copies, waits for them, and re-layouts  4.99 us (3%)
  starting transfers between devices  4.31 us (2%)
    all_gather x1, waiting for transfers between devices, per_device(): full_cols = lax.all_gather(own_cols, 'sp', axis=0, tiled=True)  77.3 us
    all_gather x1, waiting for transfers between devices, per_device(): lax.all_gather(tokens, 'tp', axis=1, tiled=True)  30.2 us
    psum x1, blocking collectives, per_device(): mixture = lax.psum(partial_value, 'sp')  17.9 us
    all_gather x1, blocking collectives, carried_in(): everything = lax.all_gather(x, axis)  17.7 us
    dot_general x1, matrix products, per_device(): jnp.einsum('spd,dw->spw', lax.all_gather(tokens, 'tp', axis=1, tiled=True...  5.22 us
    another operation x2, other arithmetic  5.02 us
    all_to_all x1, starting transfers between devices, per_device(): lax.all_to_all(key_bias, 'tp', split_axis=2, concat_axis=1, tiled=True)  4.23 us
  transfers between devices with their start and end apart: 3, of which 2 were waited for; matrix products, arithmetic and copies ran while one was open for 5% of the time, Pallas kernels for 0%

commit v1 on v0

v1 whole, which is shorter than its diff:
```python
import functools

import jax
import jax.numpy as jnp
from jax import lax
from jax.experimental import pallas as pl
from jax.experimental.pallas import tpu as pltpu
from jax.sharding import PartitionSpec as P


BF16 = jnp.bfloat16
F32 = jnp.float32


def wrapped(value, count):
    value = jnp.where(value < 0, value + count, value)
    return jnp.where(value >= count, value - count, value)


def ring_perm(count):
    order = list(range(0, count, 2)) + list(range(1, count, 2))[::-1]
    pairs = []
    for p in range(count):
        here, there = order[p], order[(p + 1) % count]
        pairs.append((here, there))
        pairs.append((count + there, count + here))
    return pairs


def origins(slots, count):
    index, forward = lax.axis_index("sp"), lax.axis_index("gr") == 0
    half = lax.shift_right_logical(index, 1)
    place = jnp.where(lax.bitwise_and(index, 1) == 0, half, count - 1 - half)
    found = []
    for slot in slots:
        away = (slot + 1) // 2 * (-1 if slot % 2 == 1 else 1)
        at = wrapped(place + jnp.where(forward, away, -away), count)
        found.append(jnp.where(at < count // 2, 2 * at, 2 * (count - 1 - at) + 1))
    return found


def taken(slots, count, depth, x):
    if count == 1:
        return x[...]
    parts = []
    for at in origins(slots, count):
        at = pl.multiple_of(at * depth, depth)
        parts.append(x[:, pl.ds(at, depth)])
    return parts[0] if len(parts) == 1 else jnp.concatenate(parts, axis=1)


def stacked(refs):
    parts = [ref[...] for ref in refs]
    return parts[0] if len(parts) == 1 else jnp.concatenate(parts, axis=0)


def dot(x, w):
    return jnp.dot(x, w, preferred_element_type=F32)


def early_kernel(count, total, depth, x, *refs):
    part = taken(range(count), total, depth, x)
    for i in range(2):
        refs[2 * count][i] = dot(part, stacked(refs[i * count : (i + 1) * count]))


def middle_kernel(tp_count, early, count, total, depth, before, *refs):
    toks, refs = refs[:tp_count], refs[tp_count:]
    weights, acc = (refs[:count], refs[count : 2 * count]), refs[2 * count]
    rows = before.shape[1]
    for t in range(tp_count):
        start = early if t == 0 else 0
        part = taken(range(start, count), total, depth, toks[t])
        for i in range(2):
            product = dot(part, stacked(weights[i][start:]))
            if t == 0:
                product += before[i]
            acc[i, t * rows : (t + 1) * rows] = product


def attend_kernel(sizes, query, offset, *refs):
    tp_count, early, slots, count, seqs, pos, depth, cols, heads, head_dim = sizes
    acc, refs = (refs[0], refs[1:]) if early else (None, refs)
    toks, refs = refs[:tp_count], refs[tp_count:]
    first, second = refs[: len(slots)], refs[len(slots) : 2 * len(slots)]
    biases, (keys, values, bias_out, stat_out, bias) = (
        refs[2 * len(slots) : -5],
        refs[-5:],
    )
    span = tp_count * pos
    rows = seqs * pos
    swapped = lax.axis_index("gr") != 0
    me_tp = lax.axis_index("tp")
    for t in range(tp_count):
        part = taken(slots, count, depth, toks[t])
        one, two = dot(part, stacked(first)), dot(part, stacked(second))
        if early:
            one += acc[0, t * rows : (t + 1) * rows]
            two += acc[1, t * rows : (t + 1) * rows]
        start = pl.multiple_of(wrapped(me_tp + t, tp_count) * pos, pos)
        for s in range(seqs):
            piece = slice(s * pos, (s + 1) * pos)
            keys[s, pl.ds(start, pos), :] = jnp.where(swapped, two[piece], one[piece]).astype(BF16)
            values[s, pl.ds(start, pos), :] = jnp.where(swapped, one[piece], two[piece]).astype(BF16)
        for s in range(seqs):
            part = biases[t][s].astype(F32)
            bias[s * heads : (s + 1) * heads, pl.ds(start, pos)] = part + offset[...]
            bias_out[s, :, pl.ds(start, pos)] = biases[t][s]
    lane_head = lax.broadcasted_iota(jnp.int32, (heads, cols), 1) // head_dim
    own_head = lane_head == lax.broadcasted_iota(jnp.int32, (heads, cols), 0)
    logits = []
    for s in range(seqs):
        q = jnp.where(own_head, jnp.broadcast_to(query[s : s + 1], (heads, cols)), 0).astype(BF16)
        logits.append(
            lax.dot_general(q, keys[s], (((1,), (1,)), ((), ())), preferred_element_type=F32)
        )
    logits = jnp.concatenate(logits, axis=0) * (head_dim**-0.5) + bias[...]
    soft = jnp.log1p(jnp.exp(-jnp.abs(logits)))
    fading = -jnp.maximum(logits, 0.0) - soft
    rising = jnp.minimum(logits, 0.0) - soft
    above = lax.broadcasted_iota(jnp.int32, (span, span), 0) > lax.broadcasted_iota(
        jnp.int32, (span, span), 1
    )
    within = jnp.dot(
        fading,
        jnp.where(above, 1.0, 0.0).astype(F32),
        preferred_element_type=F32,
        precision=lax.Precision.HIGHEST,
    )
    total = within[:, :1] + fading[:, :1]
    weights = jnp.exp(rising + within)
    high = weights.astype(BF16)
    low = (weights - high.astype(F32)).astype(BF16)
    for s in range(seqs):
        mine = slice(s * heads, (s + 1) * heads)
        spread = dot(jnp.concatenate([high[mine], low[mine]], axis=0), values[s])
        spread = spread[:heads] + spread[heads:]
        stat_out[0, s : s + 1] = jnp.sum(jnp.where(own_head, spread, 0.0), axis=0, keepdims=True)
        totals = jnp.where(own_head, jnp.broadcast_to(total[mine], (heads, cols)), 0.0)
        stat_out[1, s : s + 1] = jnp.sum(totals, axis=0, keepdims=True)


def first_kernel(cols, keys, values, first, sem):
    at = pl.ds(pl.multiple_of(lax.axis_index("tp") * cols, cols), cols)
    source = [pltpu.make_async_copy(w.at[:, at], first, sem) for w in (keys, values)]
    forward = lax.axis_index("gr") == 0
    pl.when(forward)(source[0].start)
    pl.when(jnp.logical_not(forward))(source[1].start)
    source[0].wait()


def second_kernel(sizes, keys, values, tokens, queries, offsets, biases, *refs):
    tp_count, heads, cols = sizes
    second, rows, query, offset = refs[:4]
    parts, (offsets_here, biases_here, sems) = refs[4:-3], refs[-3:]
    me = lax.axis_index("tp")
    at = pl.ds(pl.multiple_of(me * cols, cols), cols)
    source = [pltpu.make_async_copy(w.at[:, at], second, sems.at[0]) for w in (values, keys)]
    forward = lax.axis_index("gr") == 0
    pl.when(forward)(source[0].start)
    pl.when(jnp.logical_not(forward))(source[1].start)
    copies = [
        pltpu.make_async_copy(biases, biases_here, sems.at[1]),
        pltpu.make_async_copy(offsets, offsets_here, sems.at[2]),
        pltpu.make_async_copy(queries.at[:, at], query, sems.at[3]),
        pltpu.make_async_copy(tokens, rows, sems.at[4]),
    ]
    for copy in copies:
        copy.start()
    copies[0].wait()
    copies[1].wait()
    shape = (heads, offsets.shape[1])
    wanted = lax.broadcasted_iota(jnp.int32, shape, 0) + me * heads
    found = lax.broadcasted_iota(jnp.int32, shape, 1) == wanted
    picked = jnp.where(found, jnp.broadcast_to(offsets_here[...], shape), 0.0)
    offset[...] = jnp.broadcast_to(jnp.sum(picked, axis=1, keepdims=True), offset.shape)
    every = biases_here[...].astype(F32)
    for t, part in enumerate(parts):
        target = wrapped(me - t, tp_count)
        chosen = every[:, :heads]
        for n in range(1, tp_count):
            chosen = jnp.where(target == n, every[:, n * heads : (n + 1) * heads], chosen)
        part[...] = chosen.astype(BF16)
    source[0].wait()
    copies[2].wait()
    copies[3].wait()


def store_kernel(keys, values, bias, key_out, value_out, bias_out, sems):
    pairs = ((keys, key_out), (values, value_out), (bias, bias_out))
    copies = [pltpu.make_async_copy(a, b, sems.at[i]) for i, (a, b) in enumerate(pairs)]
    for copy in copies:
        copy.start()
    for copy in copies:
        copy.wait()


def combine_kernel(reach, head_dim, last, mine, other, out):
    first = lax.bitwise_and(lax.axis_index("sp"), reach) == 0
    mine_mix, mine_total = mine[0], mine[1]
    other_mix, other_total = other[0], other[1]
    early = jnp.where(first, mine_mix, other_mix)
    late = jnp.where(first, other_mix, mine_mix)
    fade = jnp.where(first, other_total, mine_total)
    mixture = early * jnp.exp(fade) + late
    if not last:
        out[0] = mixture
        out[1] = mine_total + other_total
        return
    square = mixture * mixture
    norms = []
    for at in range(0, mixture.shape[1], head_dim):
        mean = jnp.sum(square[:, at : at + head_dim], axis=1, keepdims=True) * (1.0 / head_dim)
        norms.append(jnp.broadcast_to(lax.rsqrt(mean + 1e-06), (mixture.shape[0], head_dim)))
    out[...] = mixture * jnp.concatenate(norms, axis=1)


VMEM = pl.BlockSpec(memory_space=pltpu.VMEM)
HBM = pl.BlockSpec(memory_space=pltpu.HBM)


def combine(stat, other, reach, head_dim, last):
    shape = stat.shape[1:] if last else stat.shape
    return pl.pallas_call(
        functools.partial(combine_kernel, reach, head_dim, last),
        out_shape=jax.ShapeDtypeStruct(shape, F32),
        in_specs=[VMEM, VMEM],
        out_specs=VMEM,
        compiler_params=pltpu.CompilerParams(vmem_limit_bytes=1 << 20),
        name="combine",
    )(stat, other)


def per_device(tokens, key_weight, value_weight, queries, head_offset, key_bias):
    seqs, pos, width = tokens.shape
    depth, kv_width = key_weight.shape
    all_heads = head_offset.shape[0]
    head_dim = kv_width // all_heads
    tp_count, sp_count = lax.axis_size("tp"), lax.axis_size("sp")
    cols = kv_width // tp_count
    heads = all_heads // tp_count
    span = tp_count * pos
    half = sp_count // 2
    shape = jax.ShapeDtypeStruct

    def params(mib, flops=0):
        return {
            "compiler_params": pltpu.CompilerParams(vmem_limit_bytes=int(mib * 2**20)),
            "cost_estimate": pl.CostEstimate(flops=flops, bytes_accessed=0, transcendentals=0),
        }

    def shift(array, step):
        perm = [((i + step) % tp_count, i) for i in range(tp_count)]
        return lax.ppermute(array, "tp", perm)

    ring = ring_perm(sp_count)

    def onward(array):
        return lax.ppermute(array, ("gr", "sp"), ring)

    def across(array):
        return lax.ppermute(array, "gr", [(0, 1), (1, 0)])

    def stay(array):
        return pltpu.with_memory_space_constraint(array, pltpu.HBM)

    flat = tokens.reshape(seqs * pos, width)
    a = pl.pallas_call(
        functools.partial(first_kernel, cols),
        out_shape=pltpu.VMEM((depth, cols), BF16),
        in_specs=[HBM] * 2,
        out_specs=VMEM,
        scratch_shapes=[pltpu.SemaphoreType.DMA],
        name="first",
        **params(1),
    )(stay(key_weight), stay(value_weight))
    b, rows, query, offset, *biases = pl.pallas_call(
        functools.partial(second_kernel, (tp_count, heads, cols)),
        out_shape=(
            pltpu.VMEM((depth, cols), BF16),
            pltpu.VMEM((seqs * pos, width), BF16),
            pltpu.VMEM((seqs, cols), BF16),
            pltpu.VMEM((heads, pos), F32),
        )
        + (pltpu.VMEM((seqs, heads, pos), BF16),) * tp_count,
        in_specs=[HBM] * 6,
        out_specs=(VMEM,) * (4 + tp_count),
        scratch_shapes=[
            pltpu.VMEM((1, all_heads), F32),
            pltpu.VMEM((seqs, all_heads, pos), BF16),
            pltpu.SemaphoreType.DMA((5,)),
        ],
        name="second",
        **params(2),
    )(
        stay(key_weight),
        stay(value_weight),
        stay(flat),
        stay(queries),
        stay(head_offset[None]),
        stay(jnp.transpose(key_bias, (0, 2, 1))),
    )
    toks = [rows] + [shift(flat, t) for t in range(1, tp_count)]
    biases = biases[:1] + [shift(biases[t], t) for t in range(1, tp_count)]
    first, second = [a], [b]
    for _ in range(1, half):
        a, b = onward(a), onward(b)
        first += [a, across(b)]
        second += [b, across(a)]
    a = onward(a)
    first.append(a)
    second.append(across(a))

    count, early, middle = sp_count, sp_count - 3, sp_count - 1
    if depth % 128:
        places = jnp.stack(origins(range(sp_count), sp_count))
        slot_of = jnp.argmax(places[None] == lax.iota(jnp.int32, sp_count)[:, None], axis=1)
        first = [jnp.stack(first)[slot_of].reshape(width, cols)]
        second = [jnp.stack(second)[slot_of].reshape(width, cols)]
        count, early, middle = 1, 0, 0

    acc = []
    if early:
        acc = pl.pallas_call(
            functools.partial(early_kernel, early, count, depth),
            out_shape=shape((2, seqs * pos, cols), F32),
            in_specs=[VMEM] * (1 + 2 * early),
            out_specs=VMEM,
            name="early",
            **params(8, 1 << 30),
        )(rows, *first[:early], *second[:early])
        acc = pl.pallas_call(
            functools.partial(middle_kernel, tp_count, early, middle, count, depth),
            out_shape=shape((2, tp_count * seqs * pos, cols), F32),
            in_specs=[VMEM] * (1 + tp_count + 2 * middle),
            out_specs=VMEM,
            name="middle",
            **params(8, 1 << 30),
        )(acc, *toks, *first[:middle], *second[:middle])
        acc = [acc]
    slots = tuple(range(middle, len(first)))
    sizes = (tp_count, early, slots, count, seqs, pos, depth, cols, heads, head_dim)
    cache = shape((seqs, span, cols), BF16)
    bias_shape = shape((seqs, heads, span), BF16)
    keys, values, bias, stat = pl.pallas_call(
        functools.partial(attend_kernel, sizes),
        out_shape=(cache, cache, bias_shape, shape((2, seqs, cols), F32)),
        in_specs=[VMEM] * (2 + len(acc) + 2 * tp_count + 2 * len(slots)),
        out_specs=(VMEM,) * 4,
        scratch_shapes=[pltpu.VMEM((seqs * heads, span), F32)],
        name="attend",
        **params(8 if early else 32, 1 << 30),
    )(query, offset, *acc, *toks, *first[middle:], *second[middle:], *biases)
    key_cache, value_cache, bias = pl.pallas_call(
        store_kernel,
        out_shape=(cache, cache, bias_shape),
        in_specs=[VMEM] * 3,
        out_specs=(HBM,) * 3,
        scratch_shapes=[pltpu.SemaphoreType.DMA((3,))],
        name="store",
        **params(1),
    )(keys, values, bias)

    reach = 1
    while reach < sp_count:
        other = lax.ppermute(stat, "sp", [(i, i ^ reach) for i in range(sp_count)])
        stat = combine(stat, other, reach, head_dim, 2 * reach == sp_count)
        reach *= 2
    return key_cache, value_cache, jnp.transpose(bias, (0, 2, 1)), stat


def solution(mesh):
    in_specs = (
        P("gr", ("sp", "tp"), None),
        P("sp", None),
        P("sp", None),
        P("gr", None),
        P(),
        P("gr", ("sp", "tp"), None),
    )
    out_specs = (P("gr", "sp", "tp"), P("gr", "sp", "tp"), P("gr", "sp", "tp"), P("gr", "tp"))
    return jax.shard_map(
        per_device, mesh=mesh, in_specs=in_specs, out_specs=out_specs, check_vma=False
    )
```

time: 180 us -> 47.9 us (0.27)
  waiting for transfers between devices: 108 us -> 18.3 us
  blocking collectives: 35.7 us -> 0 us
  starting transfers between devices: 4.31 us -> 20.9 us
  between operations: 14.2 us -> 0.74 us
  Pallas kernels: 0 us -> 7.72 us
  other arithmetic: 6.49 us -> 0 us
  matrix products: 5.64 us -> 0 us
  local copies, waits for them, and re-layouts: 4.99 us -> 0.01 us
    all_gather x2 -> x0, waiting for transfers between devices: 107 us -> none  [the longest x1 77.3 us: per_device(): full_cols = lax.all_gather(own_cols, 'sp', axis=0, tiled=True)]
    ppermute x0 -> x19, starting transfers between devices: none -> 20.9 us  [the longest x7 13.4 us: onward(): return lax.ppermute(array, ('gr', 'sp'), ring)]
    ppermute x0 -> x19, waiting for transfers between devices: none -> 18.3 us  [the longest x7 9.93 us: onward(): return lax.ppermute(array, ('gr', 'sp'), ring)]
    psum x1 -> x0, blocking collectives: 17.9 us -> none  [per_device(): mixture = lax.psum(partial_value, 'sp')]
    all_gather x1 -> x0, blocking collectives: 17.7 us -> none  [carried_in(): everything = lax.all_gather(x, axis)]
    pallas_call x0 -> x9, Pallas kernels: none -> 7.72 us  [the longest x1 1.4 us: per_device(): pl.pallas_call(functools.partial(second_kernel, (tp_count, heads, cols)),...]
    dot_general x3 -> x0, matrix products: 5.64 us -> none  [the longest x1 5.22 us: per_device(): jnp.einsum('spd,dw->spw', lax.all_gather(tokens, 'tp', axis=1, tiled=True...]
    another operation x2 -> x0, other arithmetic: 5.02 us -> none
  transfers between devices with their start and end apart: 3 -> 19, of which waited for: 2 -> 10; matrix products, arithmetic and copies ran while one was open for 5% -> 0% of each run, Pallas kernels for 0% -> 10%
where the time goes in v1:
time: 47.9 us; the launch traced here: 47.7 us
  starting transfers between devices  20.9 us (44%)
  waiting for transfers between devices  18.3 us (38%)
  Pallas kernels  7.72 us (16%)
  between operations  0.74 us (2%)
    ppermute x7, starting transfers between devices, onward(): return lax.ppermute(array, ('gr', 'sp'), ring)  13.4 us
    ppermute x7, waiting for transfers between devices, onward(): return lax.ppermute(array, ('gr', 'sp'), ring)  9.93 us
    ppermute x3, waiting for transfers between devices, per_device(): other = lax.ppermute(stat, 'sp', [(i, i ^ reach) for i in range(sp_count)])  7.29 us
    ppermute x3, starting transfers between devices, per_device(): other = lax.ppermute(stat, 'sp', [(i, i ^ reach) for i in range(sp_count)])  3.78 us
    ppermute x2, starting transfers between devices, shift(): return lax.ppermute(array, 'tp', perm)  3.24 us
    pallas_call x1, Pallas kernels, per_device(): pl.pallas_call(functools.partial(second_kernel, (tp_count, heads, cols)),...  1.4 us
    pallas_call x1, Pallas kernels, per_device(): pl.pallas_call(functools.partial(middle_kernel, tp_count, early, middle,...  1.39 us
    pallas_call x1, Pallas kernels, per_device(): pl.pallas_call(functools.partial(attend_kernel, sizes), out_shape=(cache,...  1.25 us
  transfers between devices with their start and end apart: 19, of which 10 were waited for; matrix products, arithmetic and copies ran while one was open for 0% of the time, Pallas kernels for 10%

profile of v1, /device:TPU:0, one launch (start us, length us, event | category | flops | bytes accessed | tf_op | source)
XLA Modules:
  0.0 47.7 jit_solution(2436112115760217249)
XLA Ops:
  1.7 3.1 %collective-permute-start = (bf16[256,512]{1,0:T(8,128)(2,1)S(1)}, bf16[256,512]{1,0:T(8,128)(2,1)S(1)}, u32[]{:S(2)}, u32[]{:S(2)}) collective-permute-start(bf16[256,512]{1,0:T(8,128)(2,1)S(1)} %first.1.refs_0_.refs_2_), channel_id=1, source_target_pairs={{0,4},{20,16},{4,8},{24,20},{8,12},{28,24},{12,14},{30,28},{14,10}... | collective-permute-start | bytes 786440 | tf_op jit(solution)/shard_map/ppermute | solution.py:259
  4.8 1.4 %second.1 = (bf16[256,512]{1,0:T(8,128)(2,1)S(1)}, bf16[256,2048]{1,0:T(8,128)(2,1)S(1)}, bf16[2,512]{1,0:T(2,128)(2,1)S(1)}, f32[8,128]{1,0:T(8,128)S(1)}, bf16...) custom-call(bf16[256,1024]{1,0:T(8,128)(2,1)} %keys.3, bf16[256,1024]{1,0:T(8,128)(2,1)} %values.3, ...), custom_call_target="tpu_custom_call" | custom-call | tf_op jit(solution)/shard_map/second/pallas_call | solution.py:277
  6.2 1.6 %collective-permute-start.1 = (bf16[256,512]{1,0:T(8,128)(2,1)S(1)}, bf16[256,512]{1,0:T(8,128)(2,1)S(1)}, u32[]{:S(2)}, u32[]{:S(2)}) collective-permute-start(bf16[256,512]{1,0:T(8,128)(2,1)S(1)} %get-tuple-element.20.refs_5_.refs_9_), channel_id=1, source_target_pairs={{0,4},{20,16},{4,8},{24,20},{8,12},{28,24},{12,14},{30,28},{14,10}... | collective-permute-start | bytes 786440 | tf_op jit(solution)/shard_map/ppermute | solution.py:259
  7.9 1.5 %collective-permute-start.8 = (bf16[256,2048]{1,0:T(8,128)(2,1)S(1)}, bf16[256,2048]{1,0:T(8,128)(2,1)S(1)}, u32[]{:S(2)}, u32[]{:S(2)}) collective-permute-start(bf16[256,2048]{1,0:T(8,128)(2,1)S(1)} %bitcast.5), channel_id=1, source_target_pairs={{1,0},{0,1},{3,2},{2,3},{5,4},{4,5},{7,6},{6,7},{9,8},{8,9},{11,10... | collective-permute-start | bytes 3145736 | tf_op jit(solution)/shard_map/ppermute | solution.py:254
  9.3 1.8 %collective-permute-start.3 = (bf16[256,512]{1,0:T(8,128)(2,1)S(1)}, bf16[256,512]{1,0:T(8,128)(2,1)S(1)}, u32[]{:S(2)}, u32[]{:S(2)}) collective-permute-start(bf16[256,512]{1,0:T(8,128)(2,1)S(1)} %collective-permute-done.refs_1_.refs_3_), channel_id=1, source_target_pairs={{0,4},{20,16},{4,8},{24,20},{8,12},{28,24},{12,14},{30,28},{14,10}... | collective-permute-start | bytes 786440 | tf_op jit(solution)/shard_map/ppermute | solution.py:259
  11.2 1.5 %collective-permute-done.1.refs_6_.refs_10_ = bf16[256,512]{1,0:T(8,128)(2,1)S(1)} collective-permute-done((bf16[256,512]{1,0:T(8,128)(2,1)S(1)}, bf16[256,512]{1,0:T(8,128)(2,1)S(1)}, u32[]{:S(2)}, u32[]{:S(2)}) %collective-permute-start.1) | collective-permute-done | bytes 262176 | tf_op jit(solution)/shard_map/ppermute | solution.py:259
  12.6 1.6 %collective-permute-start.4 = (bf16[256,512]{1,0:T(8,128)(2,1)S(1)}, bf16[256,512]{1,0:T(8,128)(2,1)S(1)}, u32[]{:S(2)}, u32[]{:S(2)}) collective-permute-start(bf16[256,512]{1,0:T(8,128)(2,1)S(1)} %collective-permute-done.1.refs_6_.refs_10_), channel_id=1, source_target_pairs={{0,4},{20,16},{4,8},{24,20},{8,12},{28,24},{12,14},{30,28},{14,10}... | collective-permute-start | bytes 786440 | tf_op jit(solution)/shard_map/ppermute | solution.py:259
  14.2 1.5 %collective-permute-done.3.refs_3_.refs_5_ = bf16[256,512]{1,0:T(8,128)(2,1)S(1)} collective-permute-done((bf16[256,512]{1,0:T(8,128)(2,1)S(1)}, bf16[256,512]{1,0:T(8,128)(2,1)S(1)}, u32[]{:S(2)}, u32[]{:S(2)}) %collective-permute-start.3) | collective-permute-done | bytes 262176 | tf_op jit(solution)/shard_map/ppermute | solution.py:259
  15.7 1.8 %collective-permute-start.9 = (bf16[256,512]{1,0:T(8,128)(2,1)S(1)}, bf16[256,512]{1,0:T(8,128)(2,1)S(1)}, u32[]{:S(2)}, u32[]{:S(2)}) collective-permute-start(bf16[256,512]{1,0:T(8,128)(2,1)S(1)} %collective-permute-done.3.refs_3_.refs_5_), channel_id=1, source_target_pairs={{0,4},{20,16},{4,8},{24,20},{8,12},{28,24},{12,14},{30,28},{14,10}... | collective-permute-start | bytes 786440 | tf_op jit(solution)/shard_map/ppermute | solution.py:259
  17.6 1.5 %collective-permute-done.4.refs_8_.refs_12_ = bf16[256,512]{1,0:T(8,128)(2,1)S(1)} collective-permute-done((bf16[256,512]{1,0:T(8,128)(2,1)S(1)}, bf16[256,512]{1,0:T(8,128)(2,1)S(1)}, u32[]{:S(2)}, u32[]{:S(2)}) %collective-permute-start.4) | collective-permute-done | bytes 262176 | tf_op jit(solution)/shard_map/ppermute | solution.py:259
  19.0 1.6 %collective-permute-start.10 = (bf16[256,512]{1,0:T(8,128)(2,1)S(1)}, bf16[256,512]{1,0:T(8,128)(2,1)S(1)}, u32[]{:S(2)}, u32[]{:S(2)}) collective-permute-start(bf16[256,512]{1,0:T(8,128)(2,1)S(1)} %collective-permute-done.4.refs_8_.refs_12_), channel_id=1, source_target_pairs={{0,4},{20,16},{4,8},{24,20},{8,12},{28,24},{12,14},{30,28},{14,10}... | collective-permute-start | bytes 786440 | tf_op jit(solution)/shard_map/ppermute | solution.py:259
  20.6 1.5 %collective-permute-done.9.refs_7_ = bf16[256,512]{1,0:T(8,128)(2,1)S(1)} collective-permute-done((bf16[256,512]{1,0:T(8,128)(2,1)S(1)}, bf16[256,512]{1,0:T(8,128)(2,1)S(1)}, u32[]{:S(2)}, u32[]{:S(2)}) %collective-permute-start.9) | collective-permute-done | bytes 262176 | tf_op jit(solution)/shard_map/ppermute | solution.py:259
  22.1 1.8 %collective-permute-start.13 = (bf16[256,512]{1,0:T(8,128)(2,1)S(1)}, bf16[256,512]{1,0:T(8,128)(2,1)S(1)}, u32[]{:S(2)}, u32[]{:S(2)}) collective-permute-start(bf16[256,512]{1,0:T(8,128)(2,1)S(1)} %collective-permute-done.9.refs_7_), channel_id=1, source_target_pairs={{0,4},{20,16},{4,8},{24,20},{8,12},{28,24},{12,14},{30,28},{14,10}... | collective-permute-start | bytes 786440 | tf_op jit(solution)/shard_map/ppermute | solution.py:259
  23.9 1.5 %collective-permute-done.10.refs_14_ = bf16[256,512]{1,0:T(8,128)(2,1)S(1)} collective-permute-done((bf16[256,512]{1,0:T(8,128)(2,1)S(1)}, bf16[256,512]{1,0:T(8,128)(2,1)S(1)}, u32[]{:S(2)}, u32[]{:S(2)}) %collective-permute-start.10) | collective-permute-done | bytes 262176 | tf_op jit(solution)/shard_map/ppermute | solution.py:259
  25.9 2.6 %collective-permute-done.13.refs_3_ = bf16[256,512]{1,0:T(8,128)(2,1)S(1)} collective-permute-done((bf16[256,512]{1,0:T(8,128)(2,1)S(1)}, bf16[256,512]{1,0:T(8,128)(2,1)S(1)}, u32[]{:S(2)}, u32[]{:S(2)}) %collective-permute-start.13) | collective-permute-done | bytes 262176 | tf_op jit(solution)/shard_map/ppermute | solution.py:259
  28.5 1.7 %collective-permute-start.15 = (bf16[2,8,128]{2,1,0:T(8,128)(2,1)S(1)}, bf16[2,8,128]{2,1,0:T(8,128)(2,1)S(1)}, u32[]{:S(2)}, u32[]{:S(2)}) collective-permute-start(bf16[2,8,128]{2,1,0:T(8,128)(2,1)S(1)} %get-tuple-element.22), channel_id=1, source_target_pairs={{1,0},{0,1},{3,2},{2,3},{5,4},{4,5},{7,6},{6,7},{9,8},{8,9},{11,10... | collective-permute-start | bytes 12296 | tf_op jit(solution)/shard_map/ppermute | solution.py:254
  31.1 1.1 %collective-permute-done.8.refs_1_.refs_2_ = bf16[256,2048]{1,0:T(8,128)(2,1)S(1)} collective-permute-done((bf16[256,2048]{1,0:T(8,128)(2,1)S(1)}, bf16[256,2048]{1,0:T(8,128)(2,1)S(1)}, u32[]{:S(2)}, u32[]{:S(2)}) %collective-permute-start.8) | collective-permute-done | bytes 1048608 | tf_op jit(solution)/shard_map/ppermute | solution.py:254
  32.2 1.4 %middle.1.refs_0_ = f32[2,512,512]{2,1,0:T(8,128)S(1)} custom-call(f32[2,256,512]{2,1,0:T(8,128)S(1)} %early.1.before, bf16[256,2048]{1,0:T(8,128)(2,1)S(1)} %get-tuple-element.19.x.refs_0_.refs_1_, bf16[256,2048]{1,0:T(8,128)(2,1)S(1)} %collective-permute-done.8.refs_1_.refs_2_, bf16[256,512]{1,0:T(8,128)(2,1)S(1)} %first.1.refs_0_.refs_2_, ...), custom_call_target="tpu_custom_call" | custom-call | flops 1073741824 | tf_op jit(solution)/shard_map/middle/pallas_call | solution.py:332
  33.6 1.2 %attend.1 = (bf16[2,256,512]{2,1,0:T(8,128)(2,1)S(1)}, bf16[2,256,512]{2,1,0:T(8,128)(2,1)S(1)}, bf16[2,8,256]{2,1,0:T(8,128)(2,1)S(1)}, f32[2,2,512]{2,1,0:T(2,128)S(1)}) custom-call(bf16[2,512]{1,0:T(2,128)(2,1)S(1)} %get-tuple-element.17.query, f32[8,128]{1,0:T(8,128)S(1)} %get-tuple-element.18.offset, f32[2,512,512]{2,1,0:T(8,128)S(1)} %middle.1.refs_0_, ...), custom_call_target="tpu_custom_call" | custom-call | flops 1073741824 | tf_op jit(solution)/shard_map/attend/pallas_call | solution.py:345
  34.9 1.6 %collective-permute-start.16 = (f32[2,2,512]{2,1,0:T(2,128)S(1)}, f32[2,2,512]{2,1,0:T(2,128)S(1)}, u32[]{:S(2)}, u32[]{:S(2)}) collective-permute-start(f32[2,2,512]{2,1,0:T(2,128)S(1)} %get-tuple-element.29.mine), channel_id=1, source_target_pairs={{0,2},{2,0},{4,6},{6,4},{8,10},{10,8},{12,14},{14,12},{1,3},{3,1},... | collective-permute-start | bytes 24584 | tf_op jit(solution)/shard_map/ppermute | solution.py:366
  36.5 2.1 %collective-permute-done.16.other = f32[2,2,512]{2,1,0:T(2,128)S(1)} collective-permute-done((f32[2,2,512]{2,1,0:T(2,128)S(1)}, f32[2,2,512]{2,1,0:T(2,128)S(1)}, u32[]{:S(2)}, u32[]{:S(2)}) %collective-permute-start.16) | collective-permute-done | bytes 8224 | tf_op jit(solution)/shard_map/ppermute | solution.py:366
  39.2 3.1 %collective-permute-done.17.other = f32[2,2,512]{2,1,0:T(2,128)S(1)} collective-permute-done((f32[2,2,512]{2,1,0:T(2,128)S(1)}, f32[2,2,512]{2,1,0:T(2,128)S(1)}, u32[]{:S(2)}, u32[]{:S(2)}) %collective-permute-start.17) | collective-permute-done | bytes 8224 | tf_op jit(solution)/shard_map/ppermute | solution.py:366
  42.3 1.6 %collective-permute-start.18 = (f32[2,2,512]{2,1,0:T(2,128)S(1)}, f32[2,2,512]{2,1,0:T(2,128)S(1)}, u32[]{:S(2)}, u32[]{:S(2)}) collective-permute-start(f32[2,2,512]{2,1,0:T(2,128)S(1)} %combine.4.mine), channel_id=1, source_target_pairs={{0,8},{2,10},{4,12},{6,14},{8,0},{10,2},{12,4},{14,6},{1,9},{3,11}... | collective-permute-start | bytes 24584 | tf_op jit(solution)/shard_map/ppermute | solution.py:366
  44.9 2.1 %collective-permute-done.18.other = f32[2,2,512]{2,1,0:T(2,128)S(1)} collective-permute-done((f32[2,2,512]{2,1,0:T(2,128)S(1)}, f32[2,2,512]{2,1,0:T(2,128)S(1)}, u32[]{:S(2)}, u32[]{:S(2)}) %collective-permute-start.18) | collective-permute-done | bytes 8224 | tf_op jit(solution)/shard_map/ppermute | solution.py:366
  (25 shorter events, 4.8 us)
Async XLA Ops:
  0.6 7.2 %copy-start = (bf16[2,128,2048]{2,1,0:T(8,128)(2,1)S(1)}, bf16[2,128,2048]{2,1,0:T(8,128)(2,1)}, u32[]{:S(2)}) copy-start(bf16[2,128,2048]{2,1,0:T(8,128)(2,1)} %param.6) | copy-start | bytes 3145732
  1.7 7.6 %collective-permute-start = (bf16[256,512]{1,0:T(8,128)(2,1)S(1)}, bf16[256,512]{1,0:T(8,128)(2,1)S(1)}, u32[]{:S(2)}, u32[]{:S(2)}) collective-permute-start(bf16[256,512]{1,0:T(8,128)(2,1)S(1)} %first.1.refs_0_.refs_2_), channel_id=1, source_target_pairs={{0,4},{20,16},{4,8},{24,20},{8,12},{28,24},{12,14},{30,28},{14,10}... | collective-permute-start | bytes 786440 | tf_op jit(solution)/shard_map/ppermute | solution.py:259
  6.2 6.4 %collective-permute-start.1 = (bf16[256,512]{1,0:T(8,128)(2,1)S(1)}, bf16[256,512]{1,0:T(8,128)(2,1)S(1)}, u32[]{:S(2)}, u32[]{:S(2)}) collective-permute-start(bf16[256,512]{1,0:T(8,128)(2,1)S(1)} %get-tuple-element.20.refs_5_.refs_9_), channel_id=1, source_target_pairs={{0,4},{20,16},{4,8},{24,20},{8,12},{28,24},{12,14},{30,28},{14,10}... | collective-permute-start | bytes 786440 | tf_op jit(solution)/shard_map/ppermute | solution.py:259
  7.9 24.3 %collective-permute-start.8 = (bf16[256,2048]{1,0:T(8,128)(2,1)S(1)}, bf16[256,2048]{1,0:T(8,128)(2,1)S(1)}, u32[]{:S(2)}, u32[]{:S(2)}) collective-permute-start(bf16[256,2048]{1,0:T(8,128)(2,1)S(1)} %bitcast.5), channel_id=1, source_target_pairs={{1,0},{0,1},{3,2},{2,3},{5,4},{4,5},{7,6},{6,7},{9,8},{8,9},{11,10... | collective-permute-start | bytes 3145736 | tf_op jit(solution)/shard_map/ppermute | solution.py:254
  9.3 6.4 %collective-permute-start.3 = (bf16[256,512]{1,0:T(8,128)(2,1)S(1)}, bf16[256,512]{1,0:T(8,128)(2,1)S(1)}, u32[]{:S(2)}, u32[]{:S(2)}) collective-permute-start(bf16[256,512]{1,0:T(8,128)(2,1)S(1)} %collective-permute-done.refs_1_.refs_3_), channel_id=1, source_target_pairs={{0,4},{20,16},{4,8},{24,20},{8,12},{28,24},{12,14},{30,28},{14,10}... | collective-permute-start | bytes 786440 | tf_op jit(solution)/shard_map/ppermute | solution.py:259
  12.6 6.4 %collective-permute-start.4 = (bf16[256,512]{1,0:T(8,128)(2,1)S(1)}, bf16[256,512]{1,0:T(8,128)(2,1)S(1)}, u32[]{:S(2)}, u32[]{:S(2)}) collective-permute-start(bf16[256,512]{1,0:T(8,128)(2,1)S(1)} %collective-permute-done.1.refs_6_.refs_10_), channel_id=1, source_target_pairs={{0,4},{20,16},{4,8},{24,20},{8,12},{28,24},{12,14},{30,28},{14,10}... | collective-permute-start | bytes 786440 | tf_op jit(solution)/shard_map/ppermute | solution.py:259
  14.2 6.4 %collective-permute-start.2 = (bf16[256,512]{1,0:T(8,128)(2,1)S(1)}, bf16[256,512]{1,0:T(8,128)(2,1)S(1)}, u32[]{:S(2)}, u32[]{:S(2)}) collective-permute-start(bf16[256,512]{1,0:T(8,128)(2,1)S(1)} %collective-permute-done.1.refs_6_.refs_10_), channel_id=1, source_target_pairs={{0,16},{16,0},{1,17},{17,1},{2,18},{18,2},{3,19},{19,3},{4,20},{20... | collective-permute-start | bytes 786440 | tf_op jit(solution)/shard_map/ppermute | solution.py:262
  15.7 6.4 %collective-permute-start.9 = (bf16[256,512]{1,0:T(8,128)(2,1)S(1)}, bf16[256,512]{1,0:T(8,128)(2,1)S(1)}, u32[]{:S(2)}, u32[]{:S(2)}) collective-permute-start(bf16[256,512]{1,0:T(8,128)(2,1)S(1)} %collective-permute-done.3.refs_3_.refs_5_), channel_id=1, source_target_pairs={{0,4},{20,16},{4,8},{24,20},{8,12},{28,24},{12,14},{30,28},{14,10}... | collective-permute-start | bytes 786440 | tf_op jit(solution)/shard_map/ppermute | solution.py:259
  17.6 6.4 %collective-permute-start.6 = (bf16[256,512]{1,0:T(8,128)(2,1)S(1)}, bf16[256,512]{1,0:T(8,128)(2,1)S(1)}, u32[]{:S(2)}, u32[]{:S(2)}) collective-permute-start(bf16[256,512]{1,0:T(8,128)(2,1)S(1)} %collective-permute-done.refs_1_.refs_3_), channel_id=1, source_target_pairs={{0,16},{16,0},{1,17},{17,1},{2,18},{18,2},{3,19},{19,3},{4,20},{20... | collective-permute-start | bytes 786440 | tf_op jit(solution)/shard_map/ppermute | solution.py:262
  19.0 6.4 %collective-permute-start.10 = (bf16[256,512]{1,0:T(8,128)(2,1)S(1)}, bf16[256,512]{1,0:T(8,128)(2,1)S(1)}, u32[]{:S(2)}, u32[]{:S(2)}) collective-permute-start(bf16[256,512]{1,0:T(8,128)(2,1)S(1)} %collective-permute-done.4.refs_8_.refs_12_), channel_id=1, source_target_pairs={{0,4},{20,16},{4,8},{24,20},{8,12},{28,24},{12,14},{30,28},{14,10}... | collective-permute-start | bytes 786440 | tf_op jit(solution)/shard_map/ppermute | solution.py:259
  20.6 4.8 %collective-permute-start.5 = (bf16[256,512]{1,0:T(8,128)(2,1)S(1)}, bf16[256,512]{1,0:T(8,128)(2,1)S(1)}, u32[]{:S(2)}, u32[]{:S(2)}) collective-permute-start(bf16[256,512]{1,0:T(8,128)(2,1)S(1)} %collective-permute-done.4.refs_8_.refs_12_), channel_id=1, source_target_pairs={{0,16},{16,0},{1,17},{17,1},{2,18},{18,2},{3,19},{19,3},{4,20},{20... | collective-permute-start | bytes 786440 | tf_op jit(solution)/shard_map/ppermute | solution.py:262
  22.1 6.4 %collective-permute-start.13 = (bf16[256,512]{1,0:T(8,128)(2,1)S(1)}, bf16[256,512]{1,0:T(8,128)(2,1)S(1)}, u32[]{:S(2)}, u32[]{:S(2)}) collective-permute-start(bf16[256,512]{1,0:T(8,128)(2,1)S(1)} %collective-permute-done.9.refs_7_), channel_id=1, source_target_pairs={{0,4},{20,16},{4,8},{24,20},{8,12},{28,24},{12,14},{30,28},{14,10}... | collective-permute-start | bytes 786440 | tf_op jit(solution)/shard_map/ppermute | solution.py:259
  23.9 4.5 %collective-permute-start.7 = (bf16[256,512]{1,0:T(8,128)(2,1)S(1)}, bf16[256,512]{1,0:T(8,128)(2,1)S(1)}, u32[]{:S(2)}, u32[]{:S(2)}) collective-permute-start(bf16[256,512]{1,0:T(8,128)(2,1)S(1)} %collective-permute-done.3.refs_3_.refs_5_), channel_id=1, source_target_pairs={{0,16},{16,0},{1,17},{17,1},{2,18},{18,2},{3,19},{19,3},{4,20},{20... | collective-permute-start | bytes 786440 | tf_op jit(solution)/shard_map/ppermute | solution.py:262
  25.4 5.7 %collective-permute-start.11 = (bf16[256,512]{1,0:T(8,128)(2,1)S(1)}, bf16[256,512]{1,0:T(8,128)(2,1)S(1)}, u32[]{:S(2)}, u32[]{:S(2)}) collective-permute-start(bf16[256,512]{1,0:T(8,128)(2,1)S(1)} %collective-permute-done.10.refs_14_), channel_id=1, source_target_pairs={{0,16},{16,0},{1,17},{17,1},{2,18},{18,2},{3,19},{19,3},{4,20},{20... | collective-permute-start | bytes 786440 | tf_op jit(solution)/shard_map/ppermute | solution.py:262
  25.4 5.7 %collective-permute-start.12 = (bf16[256,512]{1,0:T(8,128)(2,1)S(1)}, bf16[256,512]{1,0:T(8,128)(2,1)S(1)}, u32[]{:S(2)}, u32[]{:S(2)}) collective-permute-start(bf16[256,512]{1,0:T(8,128)(2,1)S(1)} %collective-permute-done.9.refs_7_), channel_id=1, source_target_pairs={{0,16},{16,0},{1,17},{17,1},{2,18},{18,2},{3,19},{19,3},{4,20},{20... | collective-permute-start | bytes 786440 | tf_op jit(solution)/shard_map/ppermute | solution.py:262
  28.5 5.1 %collective-permute-start.14 = (bf16[256,512]{1,0:T(8,128)(2,1)S(1)}, bf16[256,512]{1,0:T(8,128)(2,1)S(1)}, u32[]{:S(2)}, u32[]{:S(2)}) collective-permute-start(bf16[256,512]{1,0:T(8,128)(2,1)S(1)} %collective-permute-done.13.refs_3_), channel_id=1, source_target_pairs={{0,16},{16,0},{1,17},{17,1},{2,18},{18,2},{3,19},{19,3},{4,20},{20... | collective-permute-start | bytes 786440 | tf_op jit(solution)/shard_map/ppermute | solution.py:262
  28.5 5.1 %collective-permute-start.15 = (bf16[2,8,128]{2,1,0:T(8,128)(2,1)S(1)}, bf16[2,8,128]{2,1,0:T(8,128)(2,1)S(1)}, u32[]{:S(2)}, u32[]{:S(2)}) collective-permute-start(bf16[2,8,128]{2,1,0:T(8,128)(2,1)S(1)} %get-tuple-element.22), channel_id=1, source_target_pairs={{1,0},{0,1},{3,2},{2,3},{5,4},{4,5},{7,6},{6,7},{9,8},{8,9},{11,10... | collective-permute-start | bytes 12296 | tf_op jit(solution)/shard_map/ppermute | solution.py:254
  34.9 3.7 %collective-permute-start.16 = (f32[2,2,512]{2,1,0:T(2,128)S(1)}, f32[2,2,512]{2,1,0:T(2,128)S(1)}, u32[]{:S(2)}, u32[]{:S(2)}) collective-permute-start(f32[2,2,512]{2,1,0:T(2,128)S(1)} %get-tuple-element.29.mine), channel_id=1, source_target_pairs={{0,2},{2,0},{4,6},{6,4},{8,10},{10,8},{12,14},{14,12},{1,3},{3,1},... | collective-permute-start | bytes 24584 | tf_op jit(solution)/shard_map/ppermute | solution.py:366
  38.6 3.7 %collective-permute-start.17 = (f32[2,2,512]{2,1,0:T(2,128)S(1)}, f32[2,2,512]{2,1,0:T(2,128)S(1)}, u32[]{:S(2)}, u32[]{:S(2)}) collective-permute-start(f32[2,2,512]{2,1,0:T(2,128)S(1)} %combine.3.mine), channel_id=1, source_target_pairs={{0,4},{2,6},{4,0},{6,2},{8,12},{10,14},{12,8},{14,10},{1,5},{3,7},... | collective-permute-start | bytes 24584 | tf_op jit(solution)/shard_map/ppermute | solution.py:366
  42.3 4.6 %collective-permute-start.18 = (f32[2,2,512]{2,1,0:T(2,128)S(1)}, f32[2,2,512]{2,1,0:T(2,128)S(1)}, u32[]{:S(2)}, u32[]{:S(2)}) collective-permute-start(f32[2,2,512]{2,1,0:T(2,128)S(1)} %combine.4.mine), channel_id=1, source_target_pairs={{0,8},{2,10},{4,12},{6,14},{8,0},{10,2},{12,4},{14,6},{1,9},{3,11}... | collective-permute-start | bytes 24584 | tf_op jit(solution)/shard_map/ppermute | solution.py:366

commit v2 on v1

--- a/solution.py
+++ b/solution.py
@@ -70,6 +70,9 @@
     rows = before.shape[1]
     for t in range(tp_count):
         start = early if t == 0 else 0
+        if start == count:
+            acc[:, :rows] = before[...]
+            continue
         part = taken(range(start, count), total, depth, toks[t])
         for i in range(2):
             product = dot(part, stacked(weights[i][start:]))
@@ -91,21 +94,24 @@
     rows = seqs * pos
     swapped = lax.axis_index("gr") != 0
     me_tp = lax.axis_index("tp")
+    side = swapped.astype(jnp.int32)
+    one, two = stacked(first), stacked(second)
+    weights = (jnp.where(swapped, two, one), jnp.where(swapped, one, two))
     for t in range(tp_count):
-        part = taken(slots, count, depth, toks[t])
-        one, two = dot(part, stacked(first)), dot(part, stacked(second))
-        if early:
-            one += acc[0, t * rows : (t + 1) * rows]
-            two += acc[1, t * rows : (t + 1) * rows]
         start = pl.multiple_of(wrapped(me_tp + t, tp_count) * pos, pos)
-        for s in range(seqs):
-            piece = slice(s * pos, (s + 1) * pos)
-            keys[s, pl.ds(start, pos), :] = jnp.where(swapped, two[piece], one[piece]).astype(BF16)
-            values[s, pl.ds(start, pos), :] = jnp.where(swapped, one[piece], two[piece]).astype(BF16)
         for s in range(seqs):
             part = biases[t][s].astype(F32)
             bias[s * heads : (s + 1) * heads, pl.ds(start, pos)] = part + offset[...]
             bias_out[s, :, pl.ds(start, pos)] = biases[t][s]
+    for i, (weight, target) in enumerate(zip(weights, (keys, values))):
+        for t in range(tp_count):
+            start = pl.multiple_of(wrapped(me_tp + t, tp_count) * pos, pos)
+            product = dot(taken(slots, count, depth, toks[t]), weight)
+            if early:
+                product += acc[side if i == 0 else 1 - side, t * rows : (t + 1) * rows]
+            for s in range(seqs):
+                piece = product[s * pos : (s + 1) * pos].astype(BF16)
+                target[s, pl.ds(start, pos), :] = piece
     lane_head = lax.broadcasted_iota(jnp.int32, (heads, cols), 1) // head_dim
     own_head = lane_head == lax.broadcasted_iota(jnp.int32, (heads, cols), 0)
     logits = []
@@ -121,12 +127,13 @@
     above = lax.broadcasted_iota(jnp.int32, (span, span), 0) > lax.broadcasted_iota(
         jnp.int32, (span, span), 1
     )
-    within = jnp.dot(
-        fading,
-        jnp.where(above, 1.0, 0.0).astype(F32),
-        preferred_element_type=F32,
-        precision=lax.Precision.HIGHEST,
-    )
+    parts, rest = [], fading
+    for _ in range(3):
+        parts.append(rest.astype(BF16))
+        rest = rest - parts[-1].astype(F32)
+    sums = dot(jnp.concatenate(parts, axis=0), jnp.where(above, 1.0, 0.0).astype(BF16))
+    count = seqs * heads
+    within = sums[:count] + sums[count : 2 * count] + sums[2 * count :]
     total = within[:, :1] + fading[:, :1]
     weights = jnp.exp(rising + within)
     high = weights.astype(BF16)
@@ -140,30 +147,43 @@
         stat_out[1, s : s + 1] = jnp.sum(totals, axis=0, keepdims=True)
 
 
-def first_kernel(cols, keys, values, first, sem):
+def first_kernel(cols, keys, values, first, second, sems):
     at = pl.ds(pl.multiple_of(lax.axis_index("tp") * cols, cols), cols)
-    source = [pltpu.make_async_copy(w.at[:, at], first, sem) for w in (keys, values)]
     forward = lax.axis_index("gr") == 0
-    pl.when(forward)(source[0].start)
-    pl.when(jnp.logical_not(forward))(source[1].start)
-    source[0].wait()
-
-
-def second_kernel(sizes, keys, values, tokens, queries, offsets, biases, *refs):
+
+    def copies(one, two):
+        return [
+            pltpu.make_async_copy(one.at[:, at], first, sems.at[0]),
+            pltpu.make_async_copy(two.at[:, at], second, sems.at[1]),
+        ]
+
+    ahead, back = copies(keys, values), copies(values, keys)
+
+    @pl.when(forward)
+    def _():
+        for copy in ahead:
+            copy.start()
+
+    @pl.when(jnp.logical_not(forward))
+    def _():
+        for copy in back:
+            copy.start()
+
+    for copy in ahead:
+        copy.wait()
+
+
+def second_kernel(sizes, tokens, queries, offsets, biases, *refs):
     tp_count, heads, cols = sizes
-    second, rows, query, offset = refs[:4]
-    parts, (offsets_here, biases_here, sems) = refs[4:-3], refs[-3:]
+    rows, query, offset = refs[:3]
+    parts, (offsets_here, biases_here, sems) = refs[3:-3], refs[-3:]
     me = lax.axis_index("tp")
     at = pl.ds(pl.multiple_of(me * cols, cols), cols)
-    source = [pltpu.make_async_copy(w.at[:, at], second, sems.at[0]) for w in (values, keys)]
-    forward = lax.axis_index("gr") == 0
-    pl.when(forward)(source[0].start)
-    pl.when(jnp.logical_not(forward))(source[1].start)
     copies = [
-        pltpu.make_async_copy(biases, biases_here, sems.at[1]),
-        pltpu.make_async_copy(offsets, offsets_here, sems.at[2]),
-        pltpu.make_async_copy(queries.at[:, at], query, sems.at[3]),
-        pltpu.make_async_copy(tokens, rows, sems.at[4]),
+        pltpu.make_async_copy(biases, biases_here, sems.at[0]),
+        pltpu.make_async_copy(offsets, offsets_here, sems.at[1]),
+        pltpu.make_async_copy(queries.at[:, at], query, sems.at[2]),
+        pltpu.make_async_copy(tokens, rows, sems.at[3]),
     ]
     for copy in copies:
         copy.start()
@@ -181,7 +201,6 @@
         for n in range(1, tp_count):
             chosen = jnp.where(target == n, every[:, n * heads : (n + 1) * heads], chosen)
         part[...] = chosen.astype(BF16)
-    source[0].wait()
     copies[2].wait()
     copies[3].wait()
 
@@ -195,17 +214,23 @@
         copy.wait()
 
 
-def combine_kernel(reach, head_dim, last, mine, other, out):
-    first = lax.bitwise_and(lax.axis_index("sp"), reach) == 0
-    mine_mix, mine_total = mine[0], mine[1]
-    other_mix, other_total = other[0], other[1]
-    early = jnp.where(first, mine_mix, other_mix)
-    late = jnp.where(first, other_mix, mine_mix)
-    fade = jnp.where(first, other_total, mine_total)
-    mixture = early * jnp.exp(fade) + late
+def combine_kernel(offsets, head_dim, last, *refs):
+    stats, out = refs[:-1], refs[-1]
+    index = lax.axis_index("sp")
+    places = [lax.bitwise_xor(index, offset) for offset in offsets]
+    totals = [stat[1] for stat in stats]
+    mixture = None
+    for i, stat in enumerate(stats):
+        fade = None
+        for j, total in enumerate(totals):
+            if j != i:
+                part = jnp.where(places[j] > places[i], total, 0.0)
+                fade = part if fade is None else fade + part
+        term = stat[0] * jnp.exp(fade)
+        mixture = term if mixture is None else mixture + term
     if not last:
         out[0] = mixture
-        out[1] = mine_total + other_total
+        out[1] = functools.reduce(jnp.add, totals)
         return
     square = mixture * mixture
     norms = []
@@ -219,16 +244,24 @@
 HBM = pl.BlockSpec(memory_space=pltpu.HBM)
 
 
-def combine(stat, other, reach, head_dim, last):
-    shape = stat.shape[1:] if last else stat.shape
+def combine(stats, offsets, head_dim, last):
+    shape = stats[0].shape[1:] if last else stats[0].shape
     return pl.pallas_call(
-        functools.partial(combine_kernel, reach, head_dim, last),
+        functools.partial(combine_kernel, offsets, head_dim, last),
         out_shape=jax.ShapeDtypeStruct(shape, F32),
-        in_specs=[VMEM, VMEM],
+        in_specs=[VMEM] * len(stats),
         out_specs=VMEM,
         compiler_params=pltpu.CompilerParams(vmem_limit_bytes=1 << 20),
         name="combine",
-    )(stat, other)
+    )(*stats)
+
+
+def exchanges(count):
+    found, reach = [], 1
+    while reach < count:
+        found.append((3 * reach, reach, 2 * reach) if 4 * reach <= count else (reach,))
+        reach *= 4 if 4 * reach <= count else 2
+    return found
 
 
 def per_device(tokens, key_weight, value_weight, queries, head_offset, key_bias):
@@ -265,41 +298,33 @@
         return pltpu.with_memory_space_constraint(array, pltpu.HBM)
 
     flat = tokens.reshape(seqs * pos, width)
-    a = pl.pallas_call(
+    a, b = pl.pallas_call(
         functools.partial(first_kernel, cols),
-        out_shape=pltpu.VMEM((depth, cols), BF16),
+        out_shape=(pltpu.VMEM((depth, cols), BF16),) * 2,
         in_specs=[HBM] * 2,
-        out_specs=VMEM,
-        scratch_shapes=[pltpu.SemaphoreType.DMA],
+        out_specs=(VMEM,) * 2,
+        scratch_shapes=[pltpu.SemaphoreType.DMA((2,))],
         name="first",
         **params(1),
     )(stay(key_weight), stay(value_weight))
-    b, rows, query, offset, *biases = pl.pallas_call(
+    rows, query, offset, *biases = pl.pallas_call(
         functools.partial(second_kernel, (tp_count, heads, cols)),
         out_shape=(
-            pltpu.VMEM((depth, cols), BF16),
             pltpu.VMEM((seqs * pos, width), BF16),
             pltpu.VMEM((seqs, cols), BF16),
             pltpu.VMEM((heads, pos), F32),
         )
         + (pltpu.VMEM((seqs, heads, pos), BF16),) * tp_count,
-        in_specs=[HBM] * 6,
-        out_specs=(VMEM,) * (4 + tp_count),
+        in_specs=[HBM] * 4,
+        out_specs=(VMEM,) * (3 + tp_count),
         scratch_shapes=[
             pltpu.VMEM((1, all_heads), F32),
             pltpu.VMEM((seqs, all_heads, pos), BF16),
-            pltpu.SemaphoreType.DMA((5,)),
+            pltpu.SemaphoreType.DMA((4,)),
         ],
         name="second",
         **params(2),
-    )(
-        stay(key_weight),
-        stay(value_weight),
-        stay(flat),
-        stay(queries),
-        stay(head_offset[None]),
-        stay(jnp.transpose(key_bias, (0, 2, 1))),
-    )
+    )(stay(flat), stay(queries), stay(head_offset[None]), stay(jnp.transpose(key_bias, (0, 2, 1))))
     toks = [rows] + [shift(flat, t) for t in range(1, tp_count)]
     biases = biases[:1] + [shift(biases[t], t) for t in range(1, tp_count)]
     first, second = [a], [b]
@@ -311,7 +336,7 @@
     first.append(a)
     second.append(across(a))
 
-    count, early, middle = sp_count, sp_count - 3, sp_count - 1
+    count, early, middle = sp_count, sp_count - 1, sp_count - 1
     if depth % 128:
         places = jnp.stack(origins(range(sp_count), sp_count))
         slot_of = jnp.argmax(places[None] == lax.iota(jnp.int32, sp_count)[:, None], axis=1)
@@ -361,11 +386,13 @@
         **params(1),
     )(keys, values, bias)
 
-    reach = 1
-    while reach < sp_count:
-        other = lax.ppermute(stat, "sp", [(i, i ^ reach) for i in range(sp_count)])
-        stat = combine(stat, other, reach, head_dim, 2 * reach == sp_count)
-        reach *= 2
+    stages = exchanges(sp_count)
+    for n, offsets in enumerate(stages):
+        stats = [stat]
+        for offset in offsets:
+            perm = [(i, i ^ offset) for i in range(sp_count)]
+            stats.append(lax.ppermute(stat, "sp", perm))
+        stat = combine(stats, (0,) + offsets, head_dim, n + 1 == len(stages))
     return key_cache, value_cache, jnp.transpose(bias, (0, 2, 1)), stat
 
 

time: 47.9 us -> 47.3 us (0.987)
  waiting for transfers between devices: 18.3 us -> 13.6 us
  starting transfers between devices: 20.9 us -> 25.4 us
    ppermute x3 -> x4, waiting for transfers between devices: 7.29 us -> 4.14 us  [per_device(): stats.append(lax.ppermute(stat, 'sp', perm))]
    ppermute x3 -> x4, starting transfers between devices: 3.78 us -> 6.22 us  [per_device(): stats.append(lax.ppermute(stat, 'sp', perm))]
    ppermute x7, starting transfers between devices: 13.4 us -> 15.1 us  [onward(): return lax.ppermute(array, ('gr', 'sp'), ring)]
    ppermute x2, waiting for transfers between devices: 1.09 us -> 0.01 us  [shift(): return lax.ppermute(array, 'tp', perm)]
    ppermute x7, waiting for transfers between devices: 9.93 us -> 9.42 us  [onward(): return lax.ppermute(array, ('gr', 'sp'), ring)]
    pallas_call x4 -> x3, Pallas kernels: 1.84 us -> 1.85 us  [the longest x1 1.06 us: per_device(): pl.pallas_call(functools.partial(first_kernel, cols), out_shape=(pltpu.VM...]
  transfers between devices with their start and end apart: 19 -> 20, of which waited for: 10 -> 11; matrix products, arithmetic and copies ran while one was open for 0% -> 0% of each run, Pallas kernels for 10% -> 10%
where the time goes in v2:
time: 47.3 us; the launch traced here: 47.1 us
  starting transfers between devices  25.4 us (54%)
  waiting for transfers between devices  13.6 us (29%)
  Pallas kernels  7.39 us (16%)
  between operations  0.73 us (2%)
    ppermute x7, starting transfers between devices, onward(): return lax.ppermute(array, ('gr', 'sp'), ring)  15.1 us
    ppermute x7, waiting for transfers between devices, onward(): return lax.ppermute(array, ('gr', 'sp'), ring)  9.42 us
    ppermute x4, starting transfers between devices, per_device(): stats.append(lax.ppermute(stat, 'sp', perm))  6.22 us
    ppermute x4, waiting for transfers between devices, per_device(): stats.append(lax.ppermute(stat, 'sp', perm))  4.14 us
    ppermute x2, starting transfers between devices, shift(): return lax.ppermute(array, 'tp', perm)  3.55 us
    pallas_call x1, Pallas kernels, per_device(): pl.pallas_call(functools.partial(second_kernel, (tp_count, heads, cols)),...  1.31 us
    pallas_call x1, Pallas kernels, per_device(): pl.pallas_call(functools.partial(middle_kernel, tp_count, early, middle,...  1.21 us
    pallas_call x1, Pallas kernels, per_device(): pl.pallas_call(functools.partial(early_kernel, early, count, depth), out_...  1.11 us
  transfers between devices with their start and end apart: 20, of which 11 were waited for; matrix products, arithmetic and copies ran while one was open for 0% of the time, Pallas kernels for 10%

profile of v2, /device:TPU:0, one launch (start us, length us, event | category | flops | bytes accessed | tf_op | source)
XLA Modules:
  0.0 47.1 jit_solution(13074750577322107188)
XLA Ops:
  0.6 1.1 %first.1 = (bf16[256,512]{1,0:T(8,128)(2,1)S(1)}, bf16[256,512]{1,0:T(8,128)(2,1)S(1)}) custom-call(bf16[256,1024]{1,0:T(8,128)(2,1)} %keys.1, bf16[256,1024]{1,0:T(8,128)(2,1)} %values.1), custom_call_target="tpu_custom_call" | custom-call | tf_op jit(solution)/shard_map/first/pallas_call | solution.py:301
  1.7 3.1 %collective-permute-start = (bf16[256,512]{1,0:T(8,128)(2,1)S(1)}, bf16[256,512]{1,0:T(8,128)(2,1)S(1)}, u32[]{:S(2)}, u32[]{:S(2)}) collective-permute-start(bf16[256,512]{1,0:T(8,128)(2,1)S(1)} %get-tuple-element.21.refs_0_.refs_2_), channel_id=1, source_target_pairs={{0,4},{20,16},{4,8},{24,20},{8,12},{28,24},{12,14},{30,28},{14,10}... | collective-permute-start | bytes 786440 | tf_op jit(solution)/shard_map/ppermute | solution.py:292
  4.8 1.6 %collective-permute-start.1 = (bf16[256,512]{1,0:T(8,128)(2,1)S(1)}, bf16[256,512]{1,0:T(8,128)(2,1)S(1)}, u32[]{:S(2)}, u32[]{:S(2)}) collective-permute-start(bf16[256,512]{1,0:T(8,128)(2,1)S(1)} %get-tuple-element.22.refs_7_.refs_9_), channel_id=1, source_target_pairs={{0,4},{20,16},{4,8},{24,20},{8,12},{28,24},{12,14},{30,28},{14,10}... | collective-permute-start | bytes 786440 | tf_op jit(solution)/shard_map/ppermute | solution.py:292
  6.4 1.5 %collective-permute-start.12 = (bf16[256,2048]{1,0:T(8,128)(2,1)}, bf16[256,2048]{1,0:T(8,128)(2,1)S(1)}, u32[]{:S(2)}, u32[]{:S(2)}) collective-permute-start(bf16[256,2048]{1,0:T(8,128)(2,1)} %bitcast.4), channel_id=1, source_target_pairs={{1,0},{0,1},{3,2},{2,3},{5,4},{4,5},{7,6},{6,7},{9,8},{8,9},{11,10... | collective-permute-start | bytes 3145736 | tf_op jit(solution)/shard_map/ppermute | solution.py:287
  7.9 1.2 %collective-permute-done.refs_1_.refs_3_ = bf16[256,512]{1,0:T(8,128)(2,1)S(1)} collective-permute-done((bf16[256,512]{1,0:T(8,128)(2,1)S(1)}, bf16[256,512]{1,0:T(8,128)(2,1)S(1)}, u32[]{:S(2)}, u32[]{:S(2)}) %collective-permute-start) | collective-permute-done | bytes 262176 | tf_op jit(solution)/shard_map/ppermute | solution.py:292
  9.1 2.1 %collective-permute-start.3 = (bf16[256,512]{1,0:T(8,128)(2,1)S(1)}, bf16[256,512]{1,0:T(8,128)(2,1)S(1)}, u32[]{:S(2)}, u32[]{:S(2)}) collective-permute-start(bf16[256,512]{1,0:T(8,128)(2,1)S(1)} %collective-permute-done.refs_1_.refs_3_), channel_id=1, source_target_pairs={{0,4},{20,16},{4,8},{24,20},{8,12},{28,24},{12,14},{30,28},{14,10}... | collective-permute-start | bytes 786440 | tf_op jit(solution)/shard_map/ppermute | solution.py:292
  11.9 2.1 %collective-permute-start.4 = (bf16[256,512]{1,0:T(8,128)(2,1)S(1)}, bf16[256,512]{1,0:T(8,128)(2,1)S(1)}, u32[]{:S(2)}, u32[]{:S(2)}) collective-permute-start(bf16[256,512]{1,0:T(8,128)(2,1)S(1)} %collective-permute-done.1.refs_8_.refs_10_), channel_id=1, source_target_pairs={{0,4},{20,16},{4,8},{24,20},{8,12},{28,24},{12,14},{30,28},{14,10}... | collective-permute-start | bytes 786440 | tf_op jit(solution)/shard_map/ppermute | solution.py:292
  14.0 1.5 %collective-permute-done.3.refs_3_.refs_5_ = bf16[256,512]{1,0:T(8,128)(2,1)S(1)} collective-permute-done((bf16[256,512]{1,0:T(8,128)(2,1)S(1)}, bf16[256,512]{1,0:T(8,128)(2,1)S(1)}, u32[]{:S(2)}, u32[]{:S(2)}) %collective-permute-start.3) | collective-permute-done | bytes 262176 | tf_op jit(solution)/shard_map/ppermute | solution.py:292
  15.5 2.1 %collective-permute-start.6 = (bf16[256,512]{1,0:T(8,128)(2,1)S(1)}, bf16[256,512]{1,0:T(8,128)(2,1)S(1)}, u32[]{:S(2)}, u32[]{:S(2)}) collective-permute-start(bf16[256,512]{1,0:T(8,128)(2,1)S(1)} %collective-permute-done.3.refs_3_.refs_5_), channel_id=1, source_target_pairs={{0,4},{20,16},{4,8},{24,20},{8,12},{28,24},{12,14},{30,28},{14,10}... | collective-permute-start | bytes 786440 | tf_op jit(solution)/shard_map/ppermute | solution.py:292
  18.3 2.1 %collective-permute-start.7 = (bf16[256,512]{1,0:T(8,128)(2,1)S(1)}, bf16[256,512]{1,0:T(8,128)(2,1)S(1)}, u32[]{:S(2)}, u32[]{:S(2)}) collective-permute-start(bf16[256,512]{1,0:T(8,128)(2,1)S(1)} %collective-permute-done.4.refs_10_.refs_12_), channel_id=1, source_target_pairs={{0,4},{20,16},{4,8},{24,20},{8,12},{28,24},{12,14},{30,28},{14,10}... | collective-permute-start | bytes 786440 | tf_op jit(solution)/shard_map/ppermute | solution.py:292
  20.4 1.5 %collective-permute-done.6.refs_5_.refs_7_ = bf16[256,512]{1,0:T(8,128)(2,1)S(1)} collective-permute-done((bf16[256,512]{1,0:T(8,128)(2,1)S(1)}, bf16[256,512]{1,0:T(8,128)(2,1)S(1)}, u32[]{:S(2)}, u32[]{:S(2)}) %collective-permute-start.6) | collective-permute-done | bytes 262176 | tf_op jit(solution)/shard_map/ppermute | solution.py:292
  21.8 2.1 %collective-permute-start.13 = (bf16[256,512]{1,0:T(8,128)(2,1)S(1)}, bf16[256,512]{1,0:T(8,128)(2,1)S(1)}, u32[]{:S(2)}, u32[]{:S(2)}) collective-permute-start(bf16[256,512]{1,0:T(8,128)(2,1)S(1)} %collective-permute-done.6.refs_5_.refs_7_), channel_id=1, source_target_pairs={{0,4},{20,16},{4,8},{24,20},{8,12},{28,24},{12,14},{30,28},{14,10}... | collective-permute-start | bytes 786440 | tf_op jit(solution)/shard_map/ppermute | solution.py:292
  25.2 3.0 %collective-permute-done.13.refs_3_ = bf16[256,512]{1,0:T(8,128)(2,1)S(1)} collective-permute-done((bf16[256,512]{1,0:T(8,128)(2,1)S(1)}, bf16[256,512]{1,0:T(8,128)(2,1)S(1)}, u32[]{:S(2)}, u32[]{:S(2)}) %collective-permute-start.13) | collective-permute-done | bytes 262176 | tf_op jit(solution)/shard_map/ppermute | solution.py:292
  28.2 1.3 %second.1 = (bf16[256,2048]{1,0:T(8,128)(2,1)S(1)}, bf16[2,512]{1,0:T(2,128)(2,1)S(1)}, f32[8,128]{1,0:T(8,128)S(1)}, bf16[2,8,128]{2,1,0:T(8,128)(2,1)S(1)}, bf16[2,8,128]{2,1,0:T(8,128)(2,1)S(1)}) custom-call(bf16[256,2048]{1,0:T(8,128)(2,1)} %bitcast.5, bf16[2,1024]{1,0:T(2,128)(2,1)} %queries.1, f32[1,16]{1,0:T(1,128)} %bitcast.7, ...), custom_call_target="tpu_custom_call" | custom-call | tf_op jit(solution)/shard_map/second/pallas_call | solution.py:310
  29.5 2.1 %collective-permute-start.15 = (bf16[2,8,128]{2,1,0:T(8,128)(2,1)S(1)}, bf16[2,8,128]{2,1,0:T(8,128)(2,1)S(1)}, u32[]{:S(2)}, u32[]{:S(2)}) collective-permute-start(bf16[2,8,128]{2,1,0:T(8,128)(2,1)S(1)} %get-tuple-element.24), channel_id=1, source_target_pairs={{1,0},{0,1},{3,2},{2,3},{5,4},{4,5},{7,6},{6,7},{9,8},{8,9},{11,10... | collective-permute-start | bytes 12296 | tf_op jit(solution)/shard_map/ppermute | solution.py:287
  31.6 1.1 %early.1.before = f32[2,256,512]{2,1,0:T(8,128)S(1)} custom-call(bf16[256,2048]{1,0:T(8,128)(2,1)S(1)} %get-tuple-element.20.x.refs_0_.refs_1_, bf16[256,512]{1,0:T(8,128)(2,1)S(1)} %get-tuple-element.21.refs_0_.refs_2_, bf16[256,512]{1,0:T(8,128)(2,1)S(1)} %collective-permute-done.refs_1_.refs_3_, ...), custom_call_target="tpu_custom_call" | custom-call | flops 1073741824 | tf_op jit(solution)/shard_map/early/pallas_call | solution.py:349
  32.7 1.2 %middle.1.refs_0_ = f32[2,512,512]{2,1,0:T(8,128)S(1)} custom-call(f32[2,256,512]{2,1,0:T(8,128)S(1)} %early.1.before, bf16[256,2048]{1,0:T(8,128)(2,1)S(1)} %get-tuple-element.20.x.refs_0_.refs_1_, bf16[256,2048]{1,0:T(8,128)(2,1)S(1)} %collective-permute-done.12.refs_1_.refs_2_, bf16[256,512]{1,0:T(8,128)(2,1)S(1)} %get-tuple-element.21.refs_0_.refs_2_, ...), custom_call_target="tpu_custom_call" | custom-call | flops 1073741824 | tf_op jit(solution)/shard_map/middle/pallas_call | solution.py:357
  34.0 0.9 %attend.1 = (bf16[2,256,512]{2,1,0:T(8,128)(2,1)S(1)}, bf16[2,256,512]{2,1,0:T(8,128)(2,1)S(1)}, bf16[2,8,256]{2,1,0:T(8,128)(2,1)S(1)}, f32[2,2,512]{2,1,0:T(2,128)S(1)}) custom-call(bf16[2,512]{1,0:T(2,128)(2,1)S(1)} %get-tuple-element.18.query, f32[8,128]{1,0:T(8,128)S(1)} %get-tuple-element.19.offset, f32[2,512,512]{2,1,0:T(8,128)S(1)} %middle.1.refs_0_, ...), custom_call_target="tpu_custom_call" | custom-call | flops 1073741824 | tf_op jit(solution)/shard_map/attend/pallas_call | solution.py:370
  34.9 2.6 %collective-permute-start.16 = (f32[2,2,512]{2,1,0:T(2,128)S(1)}, f32[2,2,512]{2,1,0:T(2,128)S(1)}, u32[]{:S(2)}, u32[]{:S(2)}) collective-permute-start(f32[2,2,512]{2,1,0:T(2,128)S(1)} %get-tuple-element.31.refs_0_), channel_id=1, source_target_pairs={{0,6},{2,4},{4,2},{6,0},{8,14},{10,12},{12,10},{14,8},{1,7},{3,5},... | collective-permute-start | bytes 24584 | tf_op jit(solution)/shard_map/ppermute | solution.py:394
  38.5 1.1 %collective-permute-done.16.refs_1_ = f32[2,2,512]{2,1,0:T(2,128)S(1)} collective-permute-done((f32[2,2,512]{2,1,0:T(2,128)S(1)}, f32[2,2,512]{2,1,0:T(2,128)S(1)}, u32[]{:S(2)}, u32[]{:S(2)}) %collective-permute-start.16) | collective-permute-done | bytes 8224 | tf_op jit(solution)/shard_map/ppermute | solution.py:394
  39.5 1.6 %collective-permute-done.17.refs_2_ = f32[2,2,512]{2,1,0:T(2,128)S(1)} collective-permute-done((f32[2,2,512]{2,1,0:T(2,128)S(1)}, f32[2,2,512]{2,1,0:T(2,128)S(1)}, u32[]{:S(2)}, u32[]{:S(2)}) %collective-permute-start.17) | collective-permute-done | bytes 8224 | tf_op jit(solution)/shard_map/ppermute | solution.py:394
  41.7 2.7 %collective-permute-start.19 = (f32[2,2,512]{2,1,0:T(2,128)S(1)}, f32[2,2,512]{2,1,0:T(2,128)S(1)}, u32[]{:S(2)}, u32[]{:S(2)}) collective-permute-start(f32[2,2,512]{2,1,0:T(2,128)S(1)} %combine.2.refs_0_), channel_id=1, source_target_pairs={{0,8},{2,10},{4,12},{6,14},{8,0},{10,2},{12,4},{14,6},{1,9},{3,11}... | collective-permute-start | bytes 24584 | tf_op jit(solution)/shard_map/ppermute | solution.py:394
  44.3 1.0 %store.1 = (bf16[2,256,512]{2,1,0:T(8,128)(2,1)}, bf16[2,256,512]{2,1,0:T(8,128)(2,1)}, bf16[2,8,256]{2,1,0:T(8,128)(2,1)}) custom-call(bf16[2,256,512]{2,1,0:T(8,128)(2,1)S(1)} %get-tuple-element.25.keys, bf16[2,256,512]{2,1,0:T(8,128)(2,1)S(1)} %get-tuple-element.26.values, bf16[2,8,256]{2,1,0:T(8,128)(2,1)S(1)} %get-tuple-element.27.bias), custom_call_target="tpu_custom_call" | custom-call | tf_op jit(solution)/shard_map/store/pallas_call | solution.py:379
  45.3 1.0 %collective-permute-done.19.refs_1_ = f32[2,2,512]{2,1,0:T(2,128)S(1)} collective-permute-done((f32[2,2,512]{2,1,0:T(2,128)S(1)}, f32[2,2,512]{2,1,0:T(2,128)S(1)}, u32[]{:S(2)}, u32[]{:S(2)}) %collective-permute-start.19) | collective-permute-done | bytes 8224 | tf_op jit(solution)/shard_map/ppermute | solution.py:394
  (24 shorter events, 5.0 us)
Async XLA Ops:
  1.7 7.4 %collective-permute-start = (bf16[256,512]{1,0:T(8,128)(2,1)S(1)}, bf16[256,512]{1,0:T(8,128)(2,1)S(1)}, u32[]{:S(2)}, u32[]{:S(2)}) collective-permute-start(bf16[256,512]{1,0:T(8,128)(2,1)S(1)} %get-tuple-element.21.refs_0_.refs_2_), channel_id=1, source_target_pairs={{0,4},{20,16},{4,8},{24,20},{8,12},{28,24},{12,14},{30,28},{14,10}... | collective-permute-start | bytes 786440 | tf_op jit(solution)/shard_map/ppermute | solution.py:292
  4.8 7.1 %collective-permute-start.1 = (bf16[256,512]{1,0:T(8,128)(2,1)S(1)}, bf16[256,512]{1,0:T(8,128)(2,1)S(1)}, u32[]{:S(2)}, u32[]{:S(2)}) collective-permute-start(bf16[256,512]{1,0:T(8,128)(2,1)S(1)} %get-tuple-element.22.refs_7_.refs_9_), channel_id=1, source_target_pairs={{0,4},{20,16},{4,8},{24,20},{8,12},{28,24},{12,14},{30,28},{14,10}... | collective-permute-start | bytes 786440 | tf_op jit(solution)/shard_map/ppermute | solution.py:292
  6.4 26.3 %collective-permute-start.12 = (bf16[256,2048]{1,0:T(8,128)(2,1)}, bf16[256,2048]{1,0:T(8,128)(2,1)S(1)}, u32[]{:S(2)}, u32[]{:S(2)}) collective-permute-start(bf16[256,2048]{1,0:T(8,128)(2,1)} %bitcast.4), channel_id=1, source_target_pairs={{1,0},{0,1},{3,2},{2,3},{5,4},{4,5},{7,6},{6,7},{9,8},{8,9},{11,10... | collective-permute-start | bytes 3145736 | tf_op jit(solution)/shard_map/ppermute | solution.py:287
  9.1 6.4 %collective-permute-start.3 = (bf16[256,512]{1,0:T(8,128)(2,1)S(1)}, bf16[256,512]{1,0:T(8,128)(2,1)S(1)}, u32[]{:S(2)}, u32[]{:S(2)}) collective-permute-start(bf16[256,512]{1,0:T(8,128)(2,1)S(1)} %collective-permute-done.refs_1_.refs_3_), channel_id=1, source_target_pairs={{0,4},{20,16},{4,8},{24,20},{8,12},{28,24},{12,14},{30,28},{14,10}... | collective-permute-start | bytes 786440 | tf_op jit(solution)/shard_map/ppermute | solution.py:292
  11.9 6.4 %collective-permute-start.4 = (bf16[256,512]{1,0:T(8,128)(2,1)S(1)}, bf16[256,512]{1,0:T(8,128)(2,1)S(1)}, u32[]{:S(2)}, u32[]{:S(2)}) collective-permute-start(bf16[256,512]{1,0:T(8,128)(2,1)S(1)} %collective-permute-done.1.refs_8_.refs_10_), channel_id=1, source_target_pairs={{0,4},{20,16},{4,8},{24,20},{8,12},{28,24},{12,14},{30,28},{14,10}... | collective-permute-start | bytes 786440 | tf_op jit(solution)/shard_map/ppermute | solution.py:292
  14.0 6.4 %collective-permute-start.2 = (bf16[256,512]{1,0:T(8,128)(2,1)S(1)}, bf16[256,512]{1,0:T(8,128)(2,1)S(1)}, u32[]{:S(2)}, u32[]{:S(2)}) collective-permute-start(bf16[256,512]{1,0:T(8,128)(2,1)S(1)} %collective-permute-done.1.refs_8_.refs_10_), channel_id=1, source_target_pairs={{0,16},{16,0},{1,17},{17,1},{2,18},{18,2},{3,19},{19,3},{4,20},{20... | collective-permute-start | bytes 786440 | tf_op jit(solution)/shard_map/ppermute | solution.py:295
  15.5 6.4 %collective-permute-start.6 = (bf16[256,512]{1,0:T(8,128)(2,1)S(1)}, bf16[256,512]{1,0:T(8,128)(2,1)S(1)}, u32[]{:S(2)}, u32[]{:S(2)}) collective-permute-start(bf16[256,512]{1,0:T(8,128)(2,1)S(1)} %collective-permute-done.3.refs_3_.refs_5_), channel_id=1, source_target_pairs={{0,4},{20,16},{4,8},{24,20},{8,12},{28,24},{12,14},{30,28},{14,10}... | collective-permute-start | bytes 786440 | tf_op jit(solution)/shard_map/ppermute | solution.py:292
  17.5 6.4 %collective-permute-start.9 = (bf16[256,512]{1,0:T(8,128)(2,1)S(1)}, bf16[256,512]{1,0:T(8,128)(2,1)S(1)}, u32[]{:S(2)}, u32[]{:S(2)}) collective-permute-start(bf16[256,512]{1,0:T(8,128)(2,1)S(1)} %collective-permute-done.refs_1_.refs_3_), channel_id=1, source_target_pairs={{0,16},{16,0},{1,17},{17,1},{2,18},{18,2},{3,19},{19,3},{4,20},{20... | collective-permute-start | bytes 786440 | tf_op jit(solution)/shard_map/ppermute | solution.py:295
  18.3 6.4 %collective-permute-start.7 = (bf16[256,512]{1,0:T(8,128)(2,1)S(1)}, bf16[256,512]{1,0:T(8,128)(2,1)S(1)}, u32[]{:S(2)}, u32[]{:S(2)}) collective-permute-start(bf16[256,512]{1,0:T(8,128)(2,1)S(1)} %collective-permute-done.4.refs_10_.refs_12_), channel_id=1, source_target_pairs={{0,4},{20,16},{4,8},{24,20},{8,12},{28,24},{12,14},{30,28},{14,10}... | collective-permute-start | bytes 786440 | tf_op jit(solution)/shard_map/ppermute | solution.py:292
  20.4 4.3 %collective-permute-start.10 = (bf16[256,512]{1,0:T(8,128)(2,1)S(1)}, bf16[256,512]{1,0:T(8,128)(2,1)S(1)}, u32[]{:S(2)}, u32[]{:S(2)}) collective-permute-start(bf16[256,512]{1,0:T(8,128)(2,1)S(1)} %collective-permute-done.3.refs_3_.refs_5_), channel_id=1, source_target_pairs={{0,16},{16,0},{1,17},{17,1},{2,18},{18,2},{3,19},{19,3},{4,20},{20... | collective-permute-start | bytes 786440 | tf_op jit(solution)/shard_map/ppermute | solution.py:295
  21.8 6.4 %collective-permute-start.13 = (bf16[256,512]{1,0:T(8,128)(2,1)S(1)}, bf16[256,512]{1,0:T(8,128)(2,1)S(1)}, u32[]{:S(2)}, u32[]{:S(2)}) collective-permute-start(bf16[256,512]{1,0:T(8,128)(2,1)S(1)} %collective-permute-done.6.refs_5_.refs_7_), channel_id=1, source_target_pairs={{0,4},{20,16},{4,8},{24,20},{8,12},{28,24},{12,14},{30,28},{14,10}... | collective-permute-start | bytes 786440 | tf_op jit(solution)/shard_map/ppermute | solution.py:292
  23.9 5.6 %collective-permute-start.5 = (bf16[256,512]{1,0:T(8,128)(2,1)S(1)}, bf16[256,512]{1,0:T(8,128)(2,1)S(1)}, u32[]{:S(2)}, u32[]{:S(2)}) collective-permute-start(bf16[256,512]{1,0:T(8,128)(2,1)S(1)} %collective-permute-done.4.refs_10_.refs_12_), channel_id=1, source_target_pairs={{0,16},{16,0},{1,17},{17,1},{2,18},{18,2},{3,19},{19,3},{4,20},{20... | collective-permute-start | bytes 786440 | tf_op jit(solution)/shard_map/ppermute | solution.py:295
  24.6 7.0 %collective-permute-start.11 = (bf16[256,512]{1,0:T(8,128)(2,1)S(1)}, bf16[256,512]{1,0:T(8,128)(2,1)S(1)}, u32[]{:S(2)}, u32[]{:S(2)}) collective-permute-start(bf16[256,512]{1,0:T(8,128)(2,1)S(1)} %collective-permute-done.6.refs_5_.refs_7_), channel_id=1, source_target_pairs={{0,16},{16,0},{1,17},{17,1},{2,18},{18,2},{3,19},{19,3},{4,20},{20... | collective-permute-start | bytes 786440 | tf_op jit(solution)/shard_map/ppermute | solution.py:295
  24.7 7.0 %collective-permute-start.8 = (bf16[256,512]{1,0:T(8,128)(2,1)S(1)}, bf16[256,512]{1,0:T(8,128)(2,1)S(1)}, u32[]{:S(2)}, u32[]{:S(2)}) collective-permute-start(bf16[256,512]{1,0:T(8,128)(2,1)S(1)} %collective-permute-done.7.refs_12_.refs_14_), channel_id=1, source_target_pairs={{0,16},{16,0},{1,17},{17,1},{2,18},{18,2},{3,19},{19,3},{4,20},{20... | collective-permute-start | bytes 786440 | tf_op jit(solution)/shard_map/ppermute | solution.py:295
  28.2 5.8 %collective-permute-start.14 = (bf16[256,512]{1,0:T(8,128)(2,1)S(1)}, bf16[256,512]{1,0:T(8,128)(2,1)S(1)}, u32[]{:S(2)}, u32[]{:S(2)}) collective-permute-start(bf16[256,512]{1,0:T(8,128)(2,1)S(1)} %collective-permute-done.13.refs_3_), channel_id=1, source_target_pairs={{0,16},{16,0},{1,17},{17,1},{2,18},{18,2},{3,19},{19,3},{4,20},{20... | collective-permute-start | bytes 786440 | tf_op jit(solution)/shard_map/ppermute | solution.py:295
  29.5 4.4 %collective-permute-start.15 = (bf16[2,8,128]{2,1,0:T(8,128)(2,1)S(1)}, bf16[2,8,128]{2,1,0:T(8,128)(2,1)S(1)}, u32[]{:S(2)}, u32[]{:S(2)}) collective-permute-start(bf16[2,8,128]{2,1,0:T(8,128)(2,1)S(1)} %get-tuple-element.24), channel_id=1, source_target_pairs={{1,0},{0,1},{3,2},{2,3},{5,4},{4,5},{7,6},{6,7},{9,8},{8,9},{11,10... | collective-permute-start | bytes 12296 | tf_op jit(solution)/shard_map/ppermute | solution.py:287
  34.9 4.6 %collective-permute-start.16 = (f32[2,2,512]{2,1,0:T(2,128)S(1)}, f32[2,2,512]{2,1,0:T(2,128)S(1)}, u32[]{:S(2)}, u32[]{:S(2)}) collective-permute-start(f32[2,2,512]{2,1,0:T(2,128)S(1)} %get-tuple-element.31.refs_0_), channel_id=1, source_target_pairs={{0,6},{2,4},{4,2},{6,0},{8,14},{10,12},{12,10},{14,8},{1,7},{3,5},... | collective-permute-start | bytes 24584 | tf_op jit(solution)/shard_map/ppermute | solution.py:394
  37.5 3.7 %collective-permute-start.17 = (f32[2,2,512]{2,1,0:T(2,128)S(1)}, f32[2,2,512]{2,1,0:T(2,128)S(1)}, u32[]{:S(2)}, u32[]{:S(2)}) collective-permute-start(f32[2,2,512]{2,1,0:T(2,128)S(1)} %get-tuple-element.31.refs_0_), channel_id=1, source_target_pairs={{0,2},{2,0},{4,6},{6,4},{8,10},{10,8},{12,14},{14,12},{1,3},{3,1},... | collective-permute-start | bytes 24584 | tf_op jit(solution)/shard_map/ppermute | solution.py:394
  38.0 3.7 %collective-permute-start.18 = (f32[2,2,512]{2,1,0:T(2,128)S(1)}, f32[2,2,512]{2,1,0:T(2,128)S(1)}, u32[]{:S(2)}, u32[]{:S(2)}) collective-permute-start(f32[2,2,512]{2,1,0:T(2,128)S(1)} %get-tuple-element.31.refs_0_), channel_id=1, source_target_pairs={{0,4},{2,6},{4,0},{6,2},{8,12},{10,14},{12,8},{14,10},{1,5},{3,7},... | collective-permute-start | bytes 24584 | tf_op jit(solution)/shard_map/ppermute | solution.py:394
  41.7 4.6 %collective-permute-start.19 = (f32[2,2,512]{2,1,0:T(2,128)S(1)}, f32[2,2,512]{2,1,0:T(2,128)S(1)}, u32[]{:S(2)}, u32[]{:S(2)}) collective-permute-start(f32[2,2,512]{2,1,0:T(2,128)S(1)} %combine.2.refs_0_), channel_id=1, source_target_pairs={{0,8},{2,10},{4,12},{6,14},{8,0},{10,2},{12,4},{14,6},{1,9},{3,11}... | collective-permute-start | bytes 24584 | tf_op jit(solution)/shard_map/ppermute | solution.py:394

commit v3 on v2

--- a/solution.py
+++ b/solution.py
@@ -388,11 +388,18 @@
 
     stages = exchanges(sp_count)
     for n, offsets in enumerate(stages):
-        stats = [stat]
+        crossing = n < len(stages) // 2 * 2
+        stats = [] if crossing else [stat]
+        offsets = ((0,) if crossing else ()) + offsets
         for offset in offsets:
-            perm = [(i, i ^ offset) for i in range(sp_count)]
-            stats.append(lax.ppermute(stat, "sp", perm))
-        stat = combine(stats, (0,) + offsets, head_dim, n + 1 == len(stages))
+            perm = [
+                (g * sp_count + i, (1 - g if crossing else g) * sp_count + (i ^ offset))
+                for g in range(2)
+                for i in range(sp_count)
+            ]
+            stats.append(lax.ppermute(stat, ("gr", "sp"), perm))
+        offsets = offsets if crossing else (0,) + offsets
+        stat = combine(stats, offsets, head_dim, n + 1 == len(stages))
     return key_cache, value_cache, jnp.transpose(bias, (0, 2, 1)), stat
 
 

time: 47.3 us -> 46.4 us (0.981)
  waiting for transfers between devices: 13.6 us -> 12.7 us
    ppermute x4 -> x6, waiting for transfers between devices: 4.14 us -> 3.29 us  [per_device(): stats.append(lax.ppermute(stat, ('gr', 'sp'), perm))]
    ppermute x4 -> x6, starting transfers between devices: 6.22 us -> 6.14 us  [per_device(): stats.append(lax.ppermute(stat, ('gr', 'sp'), perm))]
  transfers between devices with their start and end apart: 20 -> 22, of which waited for: 11 -> 11; matrix products, arithmetic and copies ran while one was open for 0% -> 0% of each run, Pallas kernels for 10% -> 10%
where the time goes in v3:
time: 46.4 us; the launch traced here: 46.1 us
  starting transfers between devices  25.3 us (55%)
  waiting for transfers between devices  12.7 us (27%)
  Pallas kernels  7.39 us (16%)
  between operations  0.74 us (2%)
    ppermute x7, starting transfers between devices, onward(): return lax.ppermute(array, ('gr', 'sp'), ring)  15.1 us
    ppermute x7, waiting for transfers between devices, onward(): return lax.ppermute(array, ('gr', 'sp'), ring)  9.42 us
    ppermute x6, starting transfers between devices, per_device(): stats.append(lax.ppermute(stat, ('gr', 'sp'), perm))  6.14 us
    ppermute x2, starting transfers between devices, shift(): return lax.ppermute(array, 'tp', perm)  3.55 us
    ppermute x6, waiting for transfers between devices, per_device(): stats.append(lax.ppermute(stat, ('gr', 'sp'), perm))  3.29 us
    pallas_call x1, Pallas kernels, per_device(): pl.pallas_call(functools.partial(second_kernel, (tp_count, heads, cols)),...  1.31 us
    pallas_call x1, Pallas kernels, per_device(): pl.pallas_call(functools.partial(middle_kernel, tp_count, early, middle,...  1.21 us
    pallas_call x1, Pallas kernels, per_device(): pl.pallas_call(functools.partial(early_kernel, early, count, depth), out_...  1.11 us
  transfers between devices with their start and end apart: 22, of which 11 were waited for; matrix products, arithmetic and copies ran while one was open for 0% of the time, Pallas kernels for 10%

profile of v3, /device:TPU:0, one launch (start us, length us, event | category | flops | bytes accessed | tf_op | source)
XLA Modules:
  0.0 46.1 jit_solution(7315560558924910946)
XLA Ops:
  0.6 1.1 %first.1 = (bf16[256,512]{1,0:T(8,128)(2,1)S(1)}, bf16[256,512]{1,0:T(8,128)(2,1)S(1)}) custom-call(bf16[256,1024]{1,0:T(8,128)(2,1)} %keys.1, bf16[256,1024]{1,0:T(8,128)(2,1)} %values.1), custom_call_target="tpu_custom_call" | custom-call | tf_op jit(solution)/shard_map/first/pallas_call | solution.py:301
  1.7 3.1 %collective-permute-start = (bf16[256,512]{1,0:T(8,128)(2,1)S(1)}, bf16[256,512]{1,0:T(8,128)(2,1)S(1)}, u32[]{:S(2)}, u32[]{:S(2)}) collective-permute-start(bf16[256,512]{1,0:T(8,128)(2,1)S(1)} %get-tuple-element.21.refs_0_.refs_2_), channel_id=1, source_target_pairs={{0,4},{20,16},{4,8},{24,20},{8,12},{28,24},{12,14},{30,28},{14,10}... | collective-permute-start | bytes 786440 | tf_op jit(solution)/shard_map/ppermute | solution.py:292
  4.8 1.6 %collective-permute-start.1 = (bf16[256,512]{1,0:T(8,128)(2,1)S(1)}, bf16[256,512]{1,0:T(8,128)(2,1)S(1)}, u32[]{:S(2)}, u32[]{:S(2)}) collective-permute-start(bf16[256,512]{1,0:T(8,128)(2,1)S(1)} %get-tuple-element.22.refs_7_.refs_9_), channel_id=1, source_target_pairs={{0,4},{20,16},{4,8},{24,20},{8,12},{28,24},{12,14},{30,28},{14,10}... | collective-permute-start | bytes 786440 | tf_op jit(solution)/shard_map/ppermute | solution.py:292
  6.4 1.5 %collective-permute-start.12 = (bf16[256,2048]{1,0:T(8,128)(2,1)}, bf16[256,2048]{1,0:T(8,128)(2,1)S(1)}, u32[]{:S(2)}, u32[]{:S(2)}) collective-permute-start(bf16[256,2048]{1,0:T(8,128)(2,1)} %bitcast.4), channel_id=1, source_target_pairs={{1,0},{0,1},{3,2},{2,3},{5,4},{4,5},{7,6},{6,7},{9,8},{8,9},{11,10... | collective-permute-start | bytes 3145736 | tf_op jit(solution)/shard_map/ppermute | solution.py:287
  7.9 1.2 %collective-permute-done.refs_1_.refs_3_ = bf16[256,512]{1,0:T(8,128)(2,1)S(1)} collective-permute-done((bf16[256,512]{1,0:T(8,128)(2,1)S(1)}, bf16[256,512]{1,0:T(8,128)(2,1)S(1)}, u32[]{:S(2)}, u32[]{:S(2)}) %collective-permute-start) | collective-permute-done | bytes 262176 | tf_op jit(solution)/shard_map/ppermute | solution.py:292
  9.1 2.1 %collective-permute-start.3 = (bf16[256,512]{1,0:T(8,128)(2,1)S(1)}, bf16[256,512]{1,0:T(8,128)(2,1)S(1)}, u32[]{:S(2)}, u32[]{:S(2)}) collective-permute-start(bf16[256,512]{1,0:T(8,128)(2,1)S(1)} %collective-permute-done.refs_1_.refs_3_), channel_id=1, source_target_pairs={{0,4},{20,16},{4,8},{24,20},{8,12},{28,24},{12,14},{30,28},{14,10}... | collective-permute-start | bytes 786440 | tf_op jit(solution)/shard_map/ppermute | solution.py:292
  11.9 2.1 %collective-permute-start.4 = (bf16[256,512]{1,0:T(8,128)(2,1)S(1)}, bf16[256,512]{1,0:T(8,128)(2,1)S(1)}, u32[]{:S(2)}, u32[]{:S(2)}) collective-permute-start(bf16[256,512]{1,0:T(8,128)(2,1)S(1)} %collective-permute-done.1.refs_8_.refs_10_), channel_id=1, source_target_pairs={{0,4},{20,16},{4,8},{24,20},{8,12},{28,24},{12,14},{30,28},{14,10}... | collective-permute-start | bytes 786440 | tf_op jit(solution)/shard_map/ppermute | solution.py:292
  14.0 1.5 %collective-permute-done.3.refs_3_.refs_5_ = bf16[256,512]{1,0:T(8,128)(2,1)S(1)} collective-permute-done((bf16[256,512]{1,0:T(8,128)(2,1)S(1)}, bf16[256,512]{1,0:T(8,128)(2,1)S(1)}, u32[]{:S(2)}, u32[]{:S(2)}) %collective-permute-start.3) | collective-permute-done | bytes 262176 | tf_op jit(solution)/shard_map/ppermute | solution.py:292
  15.5 2.1 %collective-permute-start.6 = (bf16[256,512]{1,0:T(8,128)(2,1)S(1)}, bf16[256,512]{1,0:T(8,128)(2,1)S(1)}, u32[]{:S(2)}, u32[]{:S(2)}) collective-permute-start(bf16[256,512]{1,0:T(8,128)(2,1)S(1)} %collective-permute-done.3.refs_3_.refs_5_), channel_id=1, source_target_pairs={{0,4},{20,16},{4,8},{24,20},{8,12},{28,24},{12,14},{30,28},{14,10}... | collective-permute-start | bytes 786440 | tf_op jit(solution)/shard_map/ppermute | solution.py:292
  18.3 2.1 %collective-permute-start.7 = (bf16[256,512]{1,0:T(8,128)(2,1)S(1)}, bf16[256,512]{1,0:T(8,128)(2,1)S(1)}, u32[]{:S(2)}, u32[]{:S(2)}) collective-permute-start(bf16[256,512]{1,0:T(8,128)(2,1)S(1)} %collective-permute-done.4.refs_10_.refs_12_), channel_id=1, source_target_pairs={{0,4},{20,16},{4,8},{24,20},{8,12},{28,24},{12,14},{30,28},{14,10}... | collective-permute-start | bytes 786440 | tf_op jit(solution)/shard_map/ppermute | solution.py:292
  20.4 1.5 %collective-permute-done.6.refs_5_.refs_7_ = bf16[256,512]{1,0:T(8,128)(2,1)S(1)} collective-permute-done((bf16[256,512]{1,0:T(8,128)(2,1)S(1)}, bf16[256,512]{1,0:T(8,128)(2,1)S(1)}, u32[]{:S(2)}, u32[]{:S(2)}) %collective-permute-start.6) | collective-permute-done | bytes 262176 | tf_op jit(solution)/shard_map/ppermute | solution.py:292
  21.8 2.1 %collective-permute-start.13 = (bf16[256,512]{1,0:T(8,128)(2,1)S(1)}, bf16[256,512]{1,0:T(8,128)(2,1)S(1)}, u32[]{:S(2)}, u32[]{:S(2)}) collective-permute-start(bf16[256,512]{1,0:T(8,128)(2,1)S(1)} %collective-permute-done.6.refs_5_.refs_7_), channel_id=1, source_target_pairs={{0,4},{20,16},{4,8},{24,20},{8,12},{28,24},{12,14},{30,28},{14,10}... | collective-permute-start | bytes 786440 | tf_op jit(solution)/shard_map/ppermute | solution.py:292
  25.2 3.0 %collective-permute-done.13.refs_3_ = bf16[256,512]{1,0:T(8,128)(2,1)S(1)} collective-permute-done((bf16[256,512]{1,0:T(8,128)(2,1)S(1)}, bf16[256,512]{1,0:T(8,128)(2,1)S(1)}, u32[]{:S(2)}, u32[]{:S(2)}) %collective-permute-start.13) | collective-permute-done | bytes 262176 | tf_op jit(solution)/shard_map/ppermute | solution.py:292
  28.2 1.3 %second.1 = (bf16[256,2048]{1,0:T(8,128)(2,1)S(1)}, bf16[2,512]{1,0:T(2,128)(2,1)S(1)}, f32[8,128]{1,0:T(8,128)S(1)}, bf16[2,8,128]{2,1,0:T(8,128)(2,1)S(1)}, bf16[2,8,128]{2,1,0:T(8,128)(2,1)S(1)}) custom-call(bf16[256,2048]{1,0:T(8,128)(2,1)} %bitcast.5, bf16[2,1024]{1,0:T(2,128)(2,1)} %queries.1, f32[1,16]{1,0:T(1,128)} %bitcast.7, ...), custom_call_target="tpu_custom_call" | custom-call | tf_op jit(solution)/shard_map/second/pallas_call | solution.py:310
  29.5 2.1 %collective-permute-start.15 = (bf16[2,8,128]{2,1,0:T(8,128)(2,1)S(1)}, bf16[2,8,128]{2,1,0:T(8,128)(2,1)S(1)}, u32[]{:S(2)}, u32[]{:S(2)}) collective-permute-start(bf16[2,8,128]{2,1,0:T(8,128)(2,1)S(1)} %get-tuple-element.24), channel_id=1, source_target_pairs={{1,0},{0,1},{3,2},{2,3},{5,4},{4,5},{7,6},{6,7},{9,8},{8,9},{11,10... | collective-permute-start | bytes 12296 | tf_op jit(solution)/shard_map/ppermute | solution.py:287
  31.6 1.1 %early.1.before = f32[2,256,512]{2,1,0:T(8,128)S(1)} custom-call(bf16[256,2048]{1,0:T(8,128)(2,1)S(1)} %get-tuple-element.20.x.refs_0_.refs_1_, bf16[256,512]{1,0:T(8,128)(2,1)S(1)} %get-tuple-element.21.refs_0_.refs_2_, bf16[256,512]{1,0:T(8,128)(2,1)S(1)} %collective-permute-done.refs_1_.refs_3_, ...), custom_call_target="tpu_custom_call" | custom-call | flops 1073741824 | tf_op jit(solution)/shard_map/early/pallas_call | solution.py:349
  32.7 1.2 %middle.1.refs_0_ = f32[2,512,512]{2,1,0:T(8,128)S(1)} custom-call(f32[2,256,512]{2,1,0:T(8,128)S(1)} %early.1.before, bf16[256,2048]{1,0:T(8,128)(2,1)S(1)} %get-tuple-element.20.x.refs_0_.refs_1_, bf16[256,2048]{1,0:T(8,128)(2,1)S(1)} %collective-permute-done.12.refs_1_.refs_2_, bf16[256,512]{1,0:T(8,128)(2,1)S(1)} %get-tuple-element.21.refs_0_.refs_2_, ...), custom_call_target="tpu_custom_call" | custom-call | flops 1073741824 | tf_op jit(solution)/shard_map/middle/pallas_call | solution.py:357
  34.0 0.9 %attend.1 = (bf16[2,256,512]{2,1,0:T(8,128)(2,1)S(1)}, bf16[2,256,512]{2,1,0:T(8,128)(2,1)S(1)}, bf16[2,8,256]{2,1,0:T(8,128)(2,1)S(1)}, f32[2,2,512]{2,1,0:T(2,128)S(1)}) custom-call(bf16[2,512]{1,0:T(2,128)(2,1)S(1)} %get-tuple-element.18.query, f32[8,128]{1,0:T(8,128)S(1)} %get-tuple-element.19.offset, f32[2,512,512]{2,1,0:T(8,128)S(1)} %middle.1.refs_0_, ...), custom_call_target="tpu_custom_call" | custom-call | flops 1073741824 | tf_op jit(solution)/shard_map/attend/pallas_call | solution.py:370
  35.2 2.4 %collective-permute-start.17 = (f32[2,2,512]{2,1,0:T(2,128)S(1)}, f32[2,2,512]{2,1,0:T(2,128)S(1)}, u32[]{:S(2)}, u32[]{:S(2)}) collective-permute-start(f32[2,2,512]{2,1,0:T(2,128)S(1)} %get-tuple-element.31), channel_id=1, source_target_pairs={{0,22},{2,20},{4,18},{6,16},{8,30},{10,28},{12,26},{14,24},{16,6},... | collective-permute-start | bytes 24584 | tf_op jit(solution)/shard_map/ppermute | solution.py:400
  38.3 0.9 %collective-permute-done.17.refs_1_ = f32[2,2,512]{2,1,0:T(2,128)S(1)} collective-permute-done((f32[2,2,512]{2,1,0:T(2,128)S(1)}, f32[2,2,512]{2,1,0:T(2,128)S(1)}, u32[]{:S(2)}, u32[]{:S(2)}) %collective-permute-start.17) | collective-permute-done | bytes 8224 | tf_op jit(solution)/shard_map/ppermute | solution.py:400
  39.2 1.5 %collective-permute-done.18.refs_2_ = f32[2,2,512]{2,1,0:T(2,128)S(1)} collective-permute-done((f32[2,2,512]{2,1,0:T(2,128)S(1)}, f32[2,2,512]{2,1,0:T(2,128)S(1)}, u32[]{:S(2)}, u32[]{:S(2)}) %collective-permute-start.18) | collective-permute-done | bytes 8224 | tf_op jit(solution)/shard_map/ppermute | solution.py:400
  41.4 2.4 %collective-permute-start.21 = (f32[2,2,512]{2,1,0:T(2,128)S(1)}, f32[2,2,512]{2,1,0:T(2,128)S(1)}, u32[]{:S(2)}, u32[]{:S(2)}) collective-permute-start(f32[2,2,512]{2,1,0:T(2,128)S(1)} %combine.2), channel_id=1, source_target_pairs={{0,24},{2,26},{4,28},{6,30},{8,16},{10,18},{12,20},{14,22},{16,8},... | collective-permute-start | bytes 24584 | tf_op jit(solution)/shard_map/ppermute | solution.py:400
  43.8 1.0 %store.1 = (bf16[2,256,512]{2,1,0:T(8,128)(2,1)}, bf16[2,256,512]{2,1,0:T(8,128)(2,1)}, bf16[2,8,256]{2,1,0:T(8,128)(2,1)}) custom-call(bf16[2,256,512]{2,1,0:T(8,128)(2,1)S(1)} %get-tuple-element.25.keys, bf16[2,256,512]{2,1,0:T(8,128)(2,1)S(1)} %get-tuple-element.26.values, bf16[2,8,256]{2,1,0:T(8,128)(2,1)S(1)} %get-tuple-element.27.bias), custom_call_target="tpu_custom_call" | custom-call | tf_op jit(solution)/shard_map/store/pallas_call | solution.py:379
  45.4 0.8 %combine.3 = f32[2,512]{1,0:T(2,128)} custom-call(f32[2,2,512]{2,1,0:T(2,128)S(1)} %collective-permute-done.20.refs_0_, f32[2,2,512]{2,1,0:T(2,128)S(1)} %collective-permute-done.21.refs_1_), custom_call_target="tpu_custom_call" | custom-call | tf_op jit(solution)/shard_map/combine/pallas_call | solution.py:249
  (28 shorter events, 5.0 us)
Async XLA Ops:
  1.7 7.4 %collective-permute-start = (bf16[256,512]{1,0:T(8,128)(2,1)S(1)}, bf16[256,512]{1,0:T(8,128)(2,1)S(1)}, u32[]{:S(2)}, u32[]{:S(2)}) collective-permute-start(bf16[256,512]{1,0:T(8,128)(2,1)S(1)} %get-tuple-element.21.refs_0_.refs_2_), channel_id=1, source_target_pairs={{0,4},{20,16},{4,8},{24,20},{8,12},{28,24},{12,14},{30,28},{14,10}... | collective-permute-start | bytes 786440 | tf_op jit(solution)/shard_map/ppermute | solution.py:292
  4.8 7.1 %collective-permute-start.1 = (bf16[256,512]{1,0:T(8,128)(2,1)S(1)}, bf16[256,512]{1,0:T(8,128)(2,1)S(1)}, u32[]{:S(2)}, u32[]{:S(2)}) collective-permute-start(bf16[256,512]{1,0:T(8,128)(2,1)S(1)} %get-tuple-element.22.refs_7_.refs_9_), channel_id=1, source_target_pairs={{0,4},{20,16},{4,8},{24,20},{8,12},{28,24},{12,14},{30,28},{14,10}... | collective-permute-start | bytes 786440 | tf_op jit(solution)/shard_map/ppermute | solution.py:292
  6.4 26.3 %collective-permute-start.12 = (bf16[256,2048]{1,0:T(8,128)(2,1)}, bf16[256,2048]{1,0:T(8,128)(2,1)S(1)}, u32[]{:S(2)}, u32[]{:S(2)}) collective-permute-start(bf16[256,2048]{1,0:T(8,128)(2,1)} %bitcast.4), channel_id=1, source_target_pairs={{1,0},{0,1},{3,2},{2,3},{5,4},{4,5},{7,6},{6,7},{9,8},{8,9},{11,10... | collective-permute-start | bytes 3145736 | tf_op jit(solution)/shard_map/ppermute | solution.py:287
  9.1 6.4 %collective-permute-start.3 = (bf16[256,512]{1,0:T(8,128)(2,1)S(1)}, bf16[256,512]{1,0:T(8,128)(2,1)S(1)}, u32[]{:S(2)}, u32[]{:S(2)}) collective-permute-start(bf16[256,512]{1,0:T(8,128)(2,1)S(1)} %collective-permute-done.refs_1_.refs_3_), channel_id=1, source_target_pairs={{0,4},{20,16},{4,8},{24,20},{8,12},{28,24},{12,14},{30,28},{14,10}... | collective-permute-start | bytes 786440 | tf_op jit(solution)/shard_map/ppermute | solution.py:292
  11.9 6.4 %collective-permute-start.4 = (bf16[256,512]{1,0:T(8,128)(2,1)S(1)}, bf16[256,512]{1,0:T(8,128)(2,1)S(1)}, u32[]{:S(2)}, u32[]{:S(2)}) collective-permute-start(bf16[256,512]{1,0:T(8,128)(2,1)S(1)} %collective-permute-done.1.refs_8_.refs_10_), channel_id=1, source_target_pairs={{0,4},{20,16},{4,8},{24,20},{8,12},{28,24},{12,14},{30,28},{14,10}... | collective-permute-start | bytes 786440 | tf_op jit(solution)/shard_map/ppermute | solution.py:292
  14.0 6.4 %collective-permute-start.2 = (bf16[256,512]{1,0:T(8,128)(2,1)S(1)}, bf16[256,512]{1,0:T(8,128)(2,1)S(1)}, u32[]{:S(2)}, u32[]{:S(2)}) collective-permute-start(bf16[256,512]{1,0:T(8,128)(2,1)S(1)} %collective-permute-done.1.refs_8_.refs_10_), channel_id=1, source_target_pairs={{0,16},{16,0},{1,17},{17,1},{2,18},{18,2},{3,19},{19,3},{4,20},{20... | collective-permute-start | bytes 786440 | tf_op jit(solution)/shard_map/ppermute | solution.py:295
  15.5 6.4 %collective-permute-start.6 = (bf16[256,512]{1,0:T(8,128)(2,1)S(1)}, bf16[256,512]{1,0:T(8,128)(2,1)S(1)}, u32[]{:S(2)}, u32[]{:S(2)}) collective-permute-start(bf16[256,512]{1,0:T(8,128)(2,1)S(1)} %collective-permute-done.3.refs_3_.refs_5_), channel_id=1, source_target_pairs={{0,4},{20,16},{4,8},{24,20},{8,12},{28,24},{12,14},{30,28},{14,10}... | collective-permute-start | bytes 786440 | tf_op jit(solution)/shard_map/ppermute | solution.py:292
  17.5 6.4 %collective-permute-start.9 = (bf16[256,512]{1,0:T(8,128)(2,1)S(1)}, bf16[256,512]{1,0:T(8,128)(2,1)S(1)}, u32[]{:S(2)}, u32[]{:S(2)}) collective-permute-start(bf16[256,512]{1,0:T(8,128)(2,1)S(1)} %collective-permute-done.refs_1_.refs_3_), channel_id=1, source_target_pairs={{0,16},{16,0},{1,17},{17,1},{2,18},{18,2},{3,19},{19,3},{4,20},{20... | collective-permute-start | bytes 786440 | tf_op jit(solution)/shard_map/ppermute | solution.py:295
  18.3 6.4 %collective-permute-start.7 = (bf16[256,512]{1,0:T(8,128)(2,1)S(1)}, bf16[256,512]{1,0:T(8,128)(2,1)S(1)}, u32[]{:S(2)}, u32[]{:S(2)}) collective-permute-start(bf16[256,512]{1,0:T(8,128)(2,1)S(1)} %collective-permute-done.4.refs_10_.refs_12_), channel_id=1, source_target_pairs={{0,4},{20,16},{4,8},{24,20},{8,12},{28,24},{12,14},{30,28},{14,10}... | collective-permute-start | bytes 786440 | tf_op jit(solution)/shard_map/ppermute | solution.py:292
  20.4 4.3 %collective-permute-start.10 = (bf16[256,512]{1,0:T(8,128)(2,1)S(1)}, bf16[256,512]{1,0:T(8,128)(2,1)S(1)}, u32[]{:S(2)}, u32[]{:S(2)}) collective-permute-start(bf16[256,512]{1,0:T(8,128)(2,1)S(1)} %collective-permute-done.3.refs_3_.refs_5_), channel_id=1, source_target_pairs={{0,16},{16,0},{1,17},{17,1},{2,18},{18,2},{3,19},{19,3},{4,20},{20... | collective-permute-start | bytes 786440 | tf_op jit(solution)/shard_map/ppermute | solution.py:295
  21.8 6.4 %collective-permute-start.13 = (bf16[256,512]{1,0:T(8,128)(2,1)S(1)}, bf16[256,512]{1,0:T(8,128)(2,1)S(1)}, u32[]{:S(2)}, u32[]{:S(2)}) collective-permute-start(bf16[256,512]{1,0:T(8,128)(2,1)S(1)} %collective-permute-done.6.refs_5_.refs_7_), channel_id=1, source_target_pairs={{0,4},{20,16},{4,8},{24,20},{8,12},{28,24},{12,14},{30,28},{14,10}... | collective-permute-start | bytes 786440 | tf_op jit(solution)/shard_map/ppermute | solution.py:292
  23.9 5.6 %collective-permute-start.5 = (bf16[256,512]{1,0:T(8,128)(2,1)S(1)}, bf16[256,512]{1,0:T(8,128)(2,1)S(1)}, u32[]{:S(2)}, u32[]{:S(2)}) collective-permute-start(bf16[256,512]{1,0:T(8,128)(2,1)S(1)} %collective-permute-done.4.refs_10_.refs_12_), channel_id=1, source_target_pairs={{0,16},{16,0},{1,17},{17,1},{2,18},{18,2},{3,19},{19,3},{4,20},{20... | collective-permute-start | bytes 786440 | tf_op jit(solution)/shard_map/ppermute | solution.py:295
  24.6 7.0 %collective-permute-start.11 = (bf16[256,512]{1,0:T(8,128)(2,1)S(1)}, bf16[256,512]{1,0:T(8,128)(2,1)S(1)}, u32[]{:S(2)}, u32[]{:S(2)}) collective-permute-start(bf16[256,512]{1,0:T(8,128)(2,1)S(1)} %collective-permute-done.6.refs_5_.refs_7_), channel_id=1, source_target_pairs={{0,16},{16,0},{1,17},{17,1},{2,18},{18,2},{3,19},{19,3},{4,20},{20... | collective-permute-start | bytes 786440 | tf_op jit(solution)/shard_map/ppermute | solution.py:295
  24.7 7.0 %collective-permute-start.8 = (bf16[256,512]{1,0:T(8,128)(2,1)S(1)}, bf16[256,512]{1,0:T(8,128)(2,1)S(1)}, u32[]{:S(2)}, u32[]{:S(2)}) collective-permute-start(bf16[256,512]{1,0:T(8,128)(2,1)S(1)} %collective-permute-done.7.refs_12_.refs_14_), channel_id=1, source_target_pairs={{0,16},{16,0},{1,17},{17,1},{2,18},{18,2},{3,19},{19,3},{4,20},{20... | collective-permute-start | bytes 786440 | tf_op jit(solution)/shard_map/ppermute | solution.py:295
  28.2 5.8 %collective-permute-start.14 = (bf16[256,512]{1,0:T(8,128)(2,1)S(1)}, bf16[256,512]{1,0:T(8,128)(2,1)S(1)}, u32[]{:S(2)}, u32[]{:S(2)}) collective-permute-start(bf16[256,512]{1,0:T(8,128)(2,1)S(1)} %collective-permute-done.13.refs_3_), channel_id=1, source_target_pairs={{0,16},{16,0},{1,17},{17,1},{2,18},{18,2},{3,19},{19,3},{4,20},{20... | collective-permute-start | bytes 786440 | tf_op jit(solution)/shard_map/ppermute | solution.py:295
  29.5 4.4 %collective-permute-start.15 = (bf16[2,8,128]{2,1,0:T(8,128)(2,1)S(1)}, bf16[2,8,128]{2,1,0:T(8,128)(2,1)S(1)}, u32[]{:S(2)}, u32[]{:S(2)}) collective-permute-start(bf16[2,8,128]{2,1,0:T(8,128)(2,1)S(1)} %get-tuple-element.24), channel_id=1, source_target_pairs={{1,0},{0,1},{3,2},{2,3},{5,4},{4,5},{7,6},{6,7},{9,8},{8,9},{11,10... | collective-permute-start | bytes 12296 | tf_op jit(solution)/shard_map/ppermute | solution.py:287
  34.9 3.4 %collective-permute-start.16 = (f32[2,2,512]{2,1,0:T(2,128)S(1)}, f32[2,2,512]{2,1,0:T(2,128)S(1)}, u32[]{:S(2)}, u32[]{:S(2)}) collective-permute-start(f32[2,2,512]{2,1,0:T(2,128)S(1)} %get-tuple-element.31), channel_id=1, source_target_pairs={{0,16},{2,18},{4,20},{6,22},{8,24},{10,26},{12,28},{14,30},{16,0},... | collective-permute-start | bytes 24584 | tf_op jit(solution)/shard_map/ppermute | solution.py:400
  35.2 4.0 %collective-permute-start.17 = (f32[2,2,512]{2,1,0:T(2,128)S(1)}, f32[2,2,512]{2,1,0:T(2,128)S(1)}, u32[]{:S(2)}, u32[]{:S(2)}) collective-permute-start(f32[2,2,512]{2,1,0:T(2,128)S(1)} %get-tuple-element.31), channel_id=1, source_target_pairs={{0,22},{2,20},{4,18},{6,16},{8,30},{10,28},{12,26},{14,24},{16,6},... | collective-permute-start | bytes 24584 | tf_op jit(solution)/shard_map/ppermute | solution.py:400
  37.6 3.1 %collective-permute-start.18 = (f32[2,2,512]{2,1,0:T(2,128)S(1)}, f32[2,2,512]{2,1,0:T(2,128)S(1)}, u32[]{:S(2)}, u32[]{:S(2)}) collective-permute-start(f32[2,2,512]{2,1,0:T(2,128)S(1)} %get-tuple-element.31), channel_id=1, source_target_pairs={{0,18},{2,16},{4,22},{6,20},{8,26},{10,24},{12,30},{14,28},{16,2},... | collective-permute-start | bytes 24584 | tf_op jit(solution)/shard_map/ppermute | solution.py:400
  38.0 3.1 %collective-permute-start.19 = (f32[2,2,512]{2,1,0:T(2,128)S(1)}, f32[2,2,512]{2,1,0:T(2,128)S(1)}, u32[]{:S(2)}, u32[]{:S(2)}) collective-permute-start(f32[2,2,512]{2,1,0:T(2,128)S(1)} %get-tuple-element.31), channel_id=1, source_target_pairs={{0,20},{2,22},{4,16},{6,18},{8,28},{10,30},{12,24},{14,26},{16,4},... | collective-permute-start | bytes 24584 | tf_op jit(solution)/shard_map/ppermute | solution.py:400
  41.1 3.8 %collective-permute-start.20 = (f32[2,2,512]{2,1,0:T(2,128)S(1)}, f32[2,2,512]{2,1,0:T(2,128)S(1)}, u32[]{:S(2)}, u32[]{:S(2)}) collective-permute-start(f32[2,2,512]{2,1,0:T(2,128)S(1)} %combine.2), channel_id=1, source_target_pairs={{0,16},{2,18},{4,20},{6,22},{8,24},{10,26},{12,28},{14,30},{16,0},... | collective-permute-start | bytes 24584 | tf_op jit(solution)/shard_map/ppermute | solution.py:400
  41.4 4.0 %collective-permute-start.21 = (f32[2,2,512]{2,1,0:T(2,128)S(1)}, f32[2,2,512]{2,1,0:T(2,128)S(1)}, u32[]{:S(2)}, u32[]{:S(2)}) collective-permute-start(f32[2,2,512]{2,1,0:T(2,128)S(1)} %combine.2), channel_id=1, source_target_pairs={{0,24},{2,26},{4,28},{6,30},{8,16},{10,18},{12,20},{14,22},{16,8},... | collective-permute-start | bytes 24584 | tf_op jit(solution)/shard_map/ppermute | solution.py:400

commit v4 on v3

--- a/solution.py
+++ b/solution.py
@@ -17,13 +17,14 @@
     return jnp.where(value >= count, value - count, value)
 
 
-def ring_perm(count):
+def ring_perm(count, step):
     order = list(range(0, count, 2)) + list(range(1, count, 2))[::-1]
+    one, two = (step - 1) % 2 * count, step % 2 * count
     pairs = []
     for p in range(count):
         here, there = order[p], order[(p + 1) % count]
-        pairs.append((here, there))
-        pairs.append((count + there, count + here))
+        pairs.append((one + here, two + there))
+        pairs.append((two + there, one + here))
     return pairs
 
 
@@ -33,7 +34,8 @@
     place = jnp.where(lax.bitwise_and(index, 1) == 0, half, count - 1 - half)
     found = []
     for slot in slots:
-        away = (slot + 1) // 2 * (-1 if slot % 2 == 1 else 1)
+        step = (slot + 1) // 2
+        away = step if (slot + step) % 2 == 0 else -step
         at = wrapped(place + jnp.where(forward, away, -away), count)
         found.append(jnp.where(at < count // 2, 2 * at, 2 * (count - 1 - at) + 1))
     return found
@@ -58,40 +60,24 @@
     return jnp.dot(x, w, preferred_element_type=F32)
 
 
-def early_kernel(count, total, depth, x, *refs):
-    part = taken(range(count), total, depth, x)
+def project_kernel(tok_count, count, total, depth, *refs):
+    toks, refs = refs[:tok_count], refs[tok_count:]
+    part = jnp.concatenate([taken(range(count), total, depth, tok) for tok in toks], axis=0)
     for i in range(2):
         refs[2 * count][i] = dot(part, stacked(refs[i * count : (i + 1) * count]))
 
 
-def middle_kernel(tp_count, early, count, total, depth, before, *refs):
-    toks, refs = refs[:tp_count], refs[tp_count:]
-    weights, acc = (refs[:count], refs[count : 2 * count]), refs[2 * count]
-    rows = before.shape[1]
-    for t in range(tp_count):
-        start = early if t == 0 else 0
-        if start == count:
-            acc[:, :rows] = before[...]
-            continue
-        part = taken(range(start, count), total, depth, toks[t])
-        for i in range(2):
-            product = dot(part, stacked(weights[i][start:]))
-            if t == 0:
-                product += before[i]
-            acc[i, t * rows : (t + 1) * rows] = product
-
-
 def attend_kernel(sizes, query, offset, *refs):
     tp_count, early, slots, count, seqs, pos, depth, cols, heads, head_dim = sizes
-    acc, refs = (refs[0], refs[1:]) if early else (None, refs)
-    toks, refs = refs[:tp_count], refs[tp_count:]
+    acc_count = 1 + (tp_count - 1) * seqs if early else 0
+    accs, refs = refs[:acc_count], refs[acc_count:]
+    toks, refs = refs[: tp_count * seqs], refs[tp_count * seqs :]
     first, second = refs[: len(slots)], refs[len(slots) : 2 * len(slots)]
     biases, (keys, values, bias_out, stat_out, bias) = (
         refs[2 * len(slots) : -5],
         refs[-5:],
     )
     span = tp_count * pos
-    rows = seqs * pos
     swapped = lax.axis_index("gr") != 0
     me_tp = lax.axis_index("tp")
     side = swapped.astype(jnp.int32)
@@ -106,12 +92,16 @@
     for i, (weight, target) in enumerate(zip(weights, (keys, values))):
         for t in range(tp_count):
             start = pl.multiple_of(wrapped(me_tp + t, tp_count) * pos, pos)
-            product = dot(taken(slots, count, depth, toks[t]), weight)
-            if early:
-                product += acc[side if i == 0 else 1 - side, t * rows : (t + 1) * rows]
+            parts = [taken(slots, count, depth, tok) for tok in toks[t * seqs : (t + 1) * seqs]]
+            product = dot(jnp.concatenate(parts, axis=0), weight)
+            at = side if i == 0 else 1 - side
             for s in range(seqs):
-                piece = product[s * pos : (s + 1) * pos].astype(BF16)
-                target[s, pl.ds(start, pos), :] = piece
+                piece = product[s * pos : (s + 1) * pos]
+                if early and t == 0:
+                    piece += accs[0][at, s * pos : (s + 1) * pos]
+                elif early:
+                    piece += accs[1 + (t - 1) * seqs + s][at]
+                target[s, pl.ds(start, pos), :] = piece.astype(BF16)
     lane_head = lax.broadcasted_iota(jnp.int32, (heads, cols), 1) // head_dim
     own_head = lane_head == lax.broadcasted_iota(jnp.int32, (heads, cols), 0)
     logits = []
@@ -147,7 +137,8 @@
         stat_out[1, s : s + 1] = jnp.sum(totals, axis=0, keepdims=True)
 
 
-def first_kernel(cols, keys, values, first, second, sems):
+def first_kernel(cols, keys, values, tokens, first, second, *refs):
+    rows, sems = refs
     at = pl.ds(pl.multiple_of(lax.axis_index("tp") * cols, cols), cols)
     forward = lax.axis_index("gr") == 0
 
@@ -158,6 +149,7 @@
         ]
 
     ahead, back = copies(keys, values), copies(values, keys)
+    tokens_in = pltpu.make_async_copy(tokens.at[0], rows, sems.at[2])
 
     @pl.when(forward)
     def _():
@@ -169,21 +161,25 @@
         for copy in back:
             copy.start()
 
+    tokens_in.start()
     for copy in ahead:
         copy.wait()
+    tokens_in.wait()
 
 
 def second_kernel(sizes, tokens, queries, offsets, biases, *refs):
     tp_count, heads, cols = sizes
-    rows, query, offset = refs[:3]
-    parts, (offsets_here, biases_here, sems) = refs[3:-3], refs[-3:]
+    query, offset = refs[:2]
+    rows, refs = refs[2 : 1 + tokens.shape[0]], refs[1 + tokens.shape[0] :]
+    parts, (offsets_here, biases_here, sems) = refs[:-3], refs[-3:]
     me = lax.axis_index("tp")
     at = pl.ds(pl.multiple_of(me * cols, cols), cols)
     copies = [
         pltpu.make_async_copy(biases, biases_here, sems.at[0]),
         pltpu.make_async_copy(offsets, offsets_here, sems.at[1]),
         pltpu.make_async_copy(queries.at[:, at], query, sems.at[2]),
-        pltpu.make_async_copy(tokens, rows, sems.at[3]),
+    ] + [
+        pltpu.make_async_copy(tokens.at[s + 1], row, sems.at[3 + s]) for s, row in enumerate(rows)
     ]
     for copy in copies:
         copy.start()
@@ -201,8 +197,8 @@
         for n in range(1, tp_count):
             chosen = jnp.where(target == n, every[:, n * heads : (n + 1) * heads], chosen)
         part[...] = chosen.astype(BF16)
-    copies[2].wait()
-    copies[3].wait()
+    for copy in copies[2:]:
+        copy.wait()
 
 
 def store_kernel(keys, values, bias, key_out, value_out, bias_out, sems):
@@ -286,10 +282,8 @@
         perm = [((i + step) % tp_count, i) for i in range(tp_count)]
         return lax.ppermute(array, "tp", perm)
 
-    ring = ring_perm(sp_count)
-
-    def onward(array):
-        return lax.ppermute(array, ("gr", "sp"), ring)
+    def onward(array, step):
+        return lax.ppermute(array, ("gr", "sp"), ring_perm(sp_count, step))
 
     def across(array):
         return lax.ppermute(array, "gr", [(0, 1), (1, 0)])
@@ -297,44 +291,51 @@
     def stay(array):
         return pltpu.with_memory_space_constraint(array, pltpu.HBM)
 
-    flat = tokens.reshape(seqs * pos, width)
-    a, b = pl.pallas_call(
+    a, b, row = pl.pallas_call(
         functools.partial(first_kernel, cols),
-        out_shape=(pltpu.VMEM((depth, cols), BF16),) * 2,
-        in_specs=[HBM] * 2,
-        out_specs=(VMEM,) * 2,
-        scratch_shapes=[pltpu.SemaphoreType.DMA((2,))],
+        out_shape=(pltpu.VMEM((depth, cols), BF16),) * 2 + (pltpu.VMEM((pos, width), BF16),),
+        in_specs=[HBM] * 3,
+        out_specs=(VMEM,) * 3,
+        scratch_shapes=[pltpu.SemaphoreType.DMA((3,))],
         name="first",
         **params(1),
-    )(stay(key_weight), stay(value_weight))
-    rows, query, offset, *biases = pl.pallas_call(
+    )(stay(key_weight), stay(value_weight), stay(tokens))
+    query, offset, *found = pl.pallas_call(
         functools.partial(second_kernel, (tp_count, heads, cols)),
         out_shape=(
-            pltpu.VMEM((seqs * pos, width), BF16),
             pltpu.VMEM((seqs, cols), BF16),
             pltpu.VMEM((heads, pos), F32),
         )
+        + (pltpu.VMEM((pos, width), BF16),) * (seqs - 1)
         + (pltpu.VMEM((seqs, heads, pos), BF16),) * tp_count,
         in_specs=[HBM] * 4,
-        out_specs=(VMEM,) * (3 + tp_count),
+        out_specs=(VMEM,) * (1 + seqs + tp_count),
         scratch_shapes=[
             pltpu.VMEM((1, all_heads), F32),
             pltpu.VMEM((seqs, all_heads, pos), BF16),
-            pltpu.SemaphoreType.DMA((4,)),
+            pltpu.SemaphoreType.DMA((2 + seqs,)),
         ],
         name="second",
         **params(2),
-    )(stay(flat), stay(queries), stay(head_offset[None]), stay(jnp.transpose(key_bias, (0, 2, 1))))
-    toks = [rows] + [shift(flat, t) for t in range(1, tp_count)]
+    )(
+        stay(tokens),
+        stay(queries),
+        stay(head_offset[None]),
+        stay(jnp.transpose(key_bias, (0, 2, 1))),
+    )
+    rows, biases = [row] + found[: seqs - 1], found[seqs - 1 :]
+    toks = [rows] + [[shift(row, t) for row in rows] for t in range(1, tp_count)]
     biases = biases[:1] + [shift(biases[t], t) for t in range(1, tp_count)]
     first, second = [a], [b]
-    for _ in range(1, half):
-        a, b = onward(a), onward(b)
-        first += [a, across(b)]
-        second += [b, across(a)]
-    a = onward(a)
-    first.append(a)
-    second.append(across(a))
+    for j in range(1, half):
+        a, b = onward(a, j), onward(b, j)
+        from_a, from_b = across(a), across(b)
+        first += [b, from_a] if j % 2 else [a, from_b]
+        second += [a, from_b] if j % 2 else [b, from_a]
+    a = onward(a, half)
+    from_a = across(a)
+    first.append(from_a if half % 2 else a)
+    second.append(a if half % 2 else from_a)
 
     count, early, middle = sp_count, sp_count - 1, sp_count - 1
     if depth % 128:
@@ -344,25 +345,21 @@
         second = [jnp.stack(second)[slot_of].reshape(width, cols)]
         count, early, middle = 1, 0, 0
 
-    acc = []
+    def project(pieces):
+        return pl.pallas_call(
+            functools.partial(project_kernel, len(pieces), early, count, depth),
+            out_shape=shape((2, len(pieces) * pos, cols), F32),
+            in_specs=[VMEM] * (len(pieces) + 2 * early),
+            out_specs=VMEM,
+            name="project",
+            **params(8, 1 << 30),
+        )(*pieces, *first[:early], *second[:early])
+
+    accs = []
     if early:
-        acc = pl.pallas_call(
-            functools.partial(early_kernel, early, count, depth),
-            out_shape=shape((2, seqs * pos, cols), F32),
-            in_specs=[VMEM] * (1 + 2 * early),
-            out_specs=VMEM,
-            name="early",
-            **params(8, 1 << 30),
-        )(rows, *first[:early], *second[:early])
-        acc = pl.pallas_call(
-            functools.partial(middle_kernel, tp_count, early, middle, count, depth),
-            out_shape=shape((2, tp_count * seqs * pos, cols), F32),
-            in_specs=[VMEM] * (1 + tp_count + 2 * middle),
-            out_specs=VMEM,
-            name="middle",
-            **params(8, 1 << 30),
-        )(acc, *toks, *first[:middle], *second[:middle])
-        acc = [acc]
+        accs.append(project(toks[0]))
+        for t in range(1, tp_count):
+            accs += [project([tok]) for tok in toks[t]]
     slots = tuple(range(middle, len(first)))
     sizes = (tp_count, early, slots, count, seqs, pos, depth, cols, heads, head_dim)
     cache = shape((seqs, span, cols), BF16)
@@ -370,12 +367,12 @@
     keys, values, bias, stat = pl.pallas_call(
         functools.partial(attend_kernel, sizes),
         out_shape=(cache, cache, bias_shape, shape((2, seqs, cols), F32)),
-        in_specs=[VMEM] * (2 + len(acc) + 2 * tp_count + 2 * len(slots)),
+        in_specs=[VMEM] * (2 + len(accs) + (1 + seqs) * tp_count + 2 * len(slots)),
         out_specs=(VMEM,) * 4,
         scratch_shapes=[pltpu.VMEM((seqs * heads, span), F32)],
         name="attend",
         **params(8 if early else 32, 1 << 30),
-    )(query, offset, *acc, *toks, *first[middle:], *second[middle:], *biases)
+    )(query, offset, *accs, *sum(toks, []), *first[middle:], *second[middle:], *biases)
     key_cache, value_cache, bias = pl.pallas_call(
         store_kernel,
         out_shape=(cache, cache, bias_shape),

time: 46.4 us -> 59.5 us (1.28)
  waiting for transfers between devices: 12.7 us -> 28.4 us
  starting transfers between devices: 25.3 us -> 22.6 us
    ppermute x2 -> x3, waiting for transfers between devices: 0.01 us -> 13.3 us  [shift(): return lax.ppermute(array, 'tp', perm)]
    ppermute x7, starting transfers between devices: 15.1 us -> 10.9 us  [onward(): return lax.ppermute(array, ('gr', 'sp'), ring_perm(sp_count, step))]
    ppermute x7, starting transfers between devices: 0.52 us -> 2.5 us  [across(): return lax.ppermute(array, 'gr', [(0, 1), (1, 0)])]
    ppermute x7, waiting for transfers between devices: 9.42 us -> 11.3 us  [onward(): return lax.ppermute(array, ('gr', 'sp'), ring_perm(sp_count, step))]
    ppermute x2 -> x3, starting transfers between devices: 3.55 us -> 3.11 us  [shift(): return lax.ppermute(array, 'tp', perm)]
    pallas_call x2 -> x3, Pallas kernels: 2.32 us -> 2.42 us  [project(): pl.pallas_call(functools.partial(project_kernel, len(pieces), early, coun...]
  transfers between devices with their start and end apart: 22 -> 23, of which waited for: 11 -> 13; matrix products, arithmetic and copies ran while one was open for 0% -> 0% of each run, Pallas kernels for 10% -> 8%
where the time goes in v4:
time: 59.5 us; the launch traced here: 59.2 us
  waiting for transfers between devices  28.4 us (48%)
  starting transfers between devices  22.6 us (38%)
  Pallas kernels  7.49 us (13%)
  between operations  0.75 us (1%)
    ppermute x3, waiting for transfers between devices, shift(): return lax.ppermute(array, 'tp', perm)  13.3 us
    ppermute x7, waiting for transfers between devices, onward(): return lax.ppermute(array, ('gr', 'sp'), ring_perm(sp_count, step))  11.3 us
    ppermute x7, starting transfers between devices, onward(): return lax.ppermute(array, ('gr', 'sp'), ring_perm(sp_count, step))  10.9 us
    ppermute x6, starting transfers between devices, per_device(): stats.append(lax.ppermute(stat, ('gr', 'sp'), perm))  6.09 us
    ppermute x6, waiting for transfers between devices, per_device(): stats.append(lax.ppermute(stat, ('gr', 'sp'), perm))  3.34 us
    ppermute x3, starting transfers between devices, shift(): return lax.ppermute(array, 'tp', perm)  3.11 us
    ppermute x7, starting transfers between devices, across(): return lax.ppermute(array, 'gr', [(0, 1), (1, 0)])  2.5 us
    pallas_call x3, Pallas kernels, project(): pl.pallas_call(functools.partial(project_kernel, len(pieces), early, coun...  2.42 us
  transfers between devices with their start and end apart: 23, of which 13 were waited for; matrix products, arithmetic and copies ran while one was open for 0% of the time, Pallas kernels for 8%

profile of v4, /device:TPU:0, one launch (start us, length us, event | category | flops | bytes accessed | tf_op | source)
XLA Modules:
  0.0 59.2 jit_solution(9763536054933289645)
XLA Ops:
  0.6 1.2 %first.1 = (bf16[256,512]{1,0:T(8,128)(2,1)S(1)}, bf16[256,512]{1,0:T(8,128)(2,1)S(1)}, bf16[128,2048]{1,0:T(8,128)(2,1)S(1)}) custom-call(bf16[256,1024]{1,0:T(8,128)(2,1)} %keys.1, bf16[256,1024]{1,0:T(8,128)(2,1)} %values.1, bf16[2,128,2048]{2,1,0:T(8,128)(2,1)} %tokens.3), custom_call_target="tpu_custom_call" | custom-call | tf_op jit(solution)/shard_map/first/pallas_call | solution.py:294
  1.9 2.6 %collective-permute-start.1 = (bf16[256,512]{1,0:T(8,128)(2,1)S(1)}, bf16[256,512]{1,0:T(8,128)(2,1)S(1)}, u32[]{:S(2)}, u32[]{:S(2)}) collective-permute-start(bf16[256,512]{1,0:T(8,128)(2,1)S(1)} %get-tuple-element.23.refs_2_.refs_1_), channel_id=1, source_target_pairs={{0,20},{20,0},{4,24},{24,4},{8,28},{28,8},{12,30},{30,12},{14,26},... | collective-permute-start | bytes 786440 | tf_op jit(solution)/shard_map/ppermute | solution.py:286
  4.5 4.0 %collective-permute-done.1.refs_10_.refs_9_ = bf16[256,512]{1,0:T(8,128)(2,1)S(1)} collective-permute-done((bf16[256,512]{1,0:T(8,128)(2,1)S(1)}, bf16[256,512]{1,0:T(8,128)(2,1)S(1)}, u32[]{:S(2)}, u32[]{:S(2)}) %collective-permute-start.1) | collective-permute-done | bytes 262176 | tf_op jit(solution)/shard_map/ppermute | solution.py:286
  8.5 2.1 %collective-permute-start.3 = (bf16[256,512]{1,0:T(8,128)(2,1)S(1)}, bf16[256,512]{1,0:T(8,128)(2,1)S(1)}, u32[]{:S(2)}, u32[]{:S(2)}) collective-permute-start(bf16[256,512]{1,0:T(8,128)(2,1)S(1)} %collective-permute-done.1.refs_10_.refs_9_), channel_id=1, source_target_pairs={{16,4},{4,16},{20,8},{8,20},{24,12},{12,24},{28,14},{14,28},{30,10... | collective-permute-start | bytes 786440 | tf_op jit(solution)/shard_map/ppermute | solution.py:286
  11.3 2.0 %collective-permute-start.4 = (bf16[256,512]{1,0:T(8,128)(2,1)S(1)}, bf16[256,512]{1,0:T(8,128)(2,1)S(1)}, u32[]{:S(2)}, u32[]{:S(2)}) collective-permute-start(bf16[256,512]{1,0:T(8,128)(2,1)S(1)} %collective-permute-done.refs_3_.refs_2_), channel_id=1, source_target_pairs={{16,4},{4,16},{20,8},{8,20},{24,12},{12,24},{28,14},{14,28},{30,10... | collective-permute-start | bytes 786440 | tf_op jit(solution)/shard_map/ppermute | solution.py:286
  13.8 1.1 %collective-permute-done.3.refs_5_.refs_4_ = bf16[256,512]{1,0:T(8,128)(2,1)S(1)} collective-permute-done((bf16[256,512]{1,0:T(8,128)(2,1)S(1)}, bf16[256,512]{1,0:T(8,128)(2,1)S(1)}, u32[]{:S(2)}, u32[]{:S(2)}) %collective-permute-start.3) | collective-permute-done | bytes 262176 | tf_op jit(solution)/shard_map/ppermute | solution.py:286
  14.9 1.7 %collective-permute-start.7 = (bf16[256,512]{1,0:T(8,128)(2,1)S(1)}, bf16[256,512]{1,0:T(8,128)(2,1)S(1)}, u32[]{:S(2)}, u32[]{:S(2)}) collective-permute-start(bf16[256,512]{1,0:T(8,128)(2,1)S(1)} %collective-permute-done.3.refs_5_.refs_4_), channel_id=1, source_target_pairs={{0,20},{20,0},{4,24},{24,4},{8,28},{28,8},{12,30},{30,12},{14,26},... | collective-permute-start | bytes 786440 | tf_op jit(solution)/shard_map/ppermute | solution.py:286
  16.6 1.1 %collective-permute-done.4.refs_12_.refs_11_ = bf16[256,512]{1,0:T(8,128)(2,1)S(1)} collective-permute-done((bf16[256,512]{1,0:T(8,128)(2,1)S(1)}, bf16[256,512]{1,0:T(8,128)(2,1)S(1)}, u32[]{:S(2)}, u32[]{:S(2)}) %collective-permute-start.4) | collective-permute-done | bytes 262176 | tf_op jit(solution)/shard_map/ppermute | solution.py:286
  17.7 1.8 %collective-permute-start.6 = (bf16[256,512]{1,0:T(8,128)(2,1)S(1)}, bf16[256,512]{1,0:T(8,128)(2,1)S(1)}, u32[]{:S(2)}, u32[]{:S(2)}) collective-permute-start(bf16[256,512]{1,0:T(8,128)(2,1)S(1)} %collective-permute-done.4.refs_12_.refs_11_), channel_id=1, source_target_pairs={{0,20},{20,0},{4,24},{24,4},{8,28},{28,8},{12,30},{30,12},{14,26},... | collective-permute-start | bytes 786440 | tf_op jit(solution)/shard_map/ppermute | solution.py:286
  20.1 1.1 %second.1 = (bf16[2,512]{1,0:T(2,128)(2,1)S(1)}, f32[8,128]{1,0:T(8,128)S(1)}, bf16[128,2048]{1,0:T(8,128)(2,1)S(1)}, bf16[2,8,128]{2,1,0:T(8,128)(2,1)S(1)}, bf16[2,8,128]{2,1,0:T(8,128)(2,1)S(1)}) custom-call(bf16[2,128,2048]{2,1,0:T(8,128)(2,1)} %tokens.3, bf16[2,1024]{1,0:T(2,128)(2,1)} %queries.1, f32[1,16]{1,0:T(1,128)} %bitcast.4, ...), custom_call_target="tpu_custom_call" | custom-call | tf_op jit(solution)/shard_map/second/pallas_call | solution.py:303
  21.2 1.6 %collective-permute-start.13 = (bf16[128,2048]{1,0:T(8,128)(2,1)S(1)}, bf16[128,2048]{1,0:T(8,128)(2,1)S(1)}, u32[]{:S(2)}, u32[]{:S(2)}) collective-permute-start(bf16[128,2048]{1,0:T(8,128)(2,1)S(1)} %get-tuple-element.22.refs_1_.refs_4_), channel_id=1, source_target_pairs={{1,0},{0,1},{3,2},{2,3},{5,4},{4,5},{7,6},{6,7},{9,8},{8,9},{11,10... | collective-permute-start | bytes 1572872 | tf_op jit(solution)/shard_map/ppermute | solution.py:283
  23.3 0.8 %collective-permute-done.6.refs_7_.refs_6_ = bf16[256,512]{1,0:T(8,128)(2,1)S(1)} collective-permute-done((bf16[256,512]{1,0:T(8,128)(2,1)S(1)}, bf16[256,512]{1,0:T(8,128)(2,1)S(1)}, u32[]{:S(2)}, u32[]{:S(2)}) %collective-permute-start.6) | collective-permute-done | bytes 262176 | tf_op jit(solution)/shard_map/ppermute | solution.py:286
  24.1 1.1 %collective-permute-start.8 = (bf16[256,512]{1,0:T(8,128)(2,1)S(1)}, bf16[256,512]{1,0:T(8,128)(2,1)S(1)}, u32[]{:S(2)}, u32[]{:S(2)}) collective-permute-start(bf16[256,512]{1,0:T(8,128)(2,1)S(1)} %collective-permute-done.7.refs_14_.refs_13_), channel_id=1, source_target_pairs={{0,16},{16,0},{1,17},{17,1},{2,18},{18,2},{3,19},{19,3},{4,20},{20... | collective-permute-start | bytes 786440 | tf_op jit(solution)/shard_map/ppermute | solution.py:289
  26.4 1.0 %collective-permute-start.16 = (bf16[2,8,128]{2,1,0:T(8,128)(2,1)S(1)}, bf16[2,8,128]{2,1,0:T(8,128)(2,1)S(1)}, u32[]{:S(2)}, u32[]{:S(2)}) collective-permute-start(bf16[2,8,128]{2,1,0:T(8,128)(2,1)S(1)} %get-tuple-element.26), channel_id=1, source_target_pairs={{1,0},{0,1},{3,2},{2,3},{5,4},{4,5},{7,6},{6,7},{9,8},{8,9},{11,10... | collective-permute-start | bytes 12296 | tf_op jit(solution)/shard_map/ppermute | solution.py:283
  27.4 3.6 %collective-permute-done.14.refs_7_ = bf16[256,512]{1,0:T(8,128)(2,1)S(1)} collective-permute-done((bf16[256,512]{1,0:T(8,128)(2,1)S(1)}, bf16[256,512]{1,0:T(8,128)(2,1)S(1)}, u32[]{:S(2)}, u32[]{:S(2)}) %collective-permute-start.14) | collective-permute-done | bytes 262176 | tf_op jit(solution)/shard_map/ppermute | solution.py:286
  31.3 1.1 %project.3.refs_0_ = f32[2,256,512]{2,1,0:T(8,128)S(1)} custom-call(bf16[128,2048]{1,0:T(8,128)(2,1)S(1)} %get-tuple-element.21.refs_0_.refs_3_, bf16[128,2048]{1,0:T(8,128)(2,1)S(1)} %get-tuple-element.22.refs_1_.refs_4_, bf16[256,512]{1,0:T(8,128)(2,1)S(1)} %get-tuple-element.23.refs_2_.refs_1_, bf16[256,512]{1,0:T(8,128)(2,1)S(1)} %collective-permute-done.refs_3_.refs_2_, ...), custom_call_target="tpu_custom_call" | custom-call | flops 1073741824 | tf_op jit(solution)/shard_map/project/pallas_call | solution.py:349
  32.4 3.6 %collective-permute-done.13.refs_0_.refs_6_ = bf16[128,2048]{1,0:T(8,128)(2,1)S(1)} collective-permute-done((bf16[128,2048]{1,0:T(8,128)(2,1)S(1)}, bf16[128,2048]{1,0:T(8,128)(2,1)S(1)}, u32[]{:S(2)}, u32[]{:S(2)}) %collective-permute-start.13) | collective-permute-done | bytes 524320 | tf_op jit(solution)/shard_map/ppermute | solution.py:283
  36.7 9.6 %collective-permute-done.12.refs_0_.refs_5_ = bf16[128,2048]{1,0:T(8,128)(2,1)S(1)} collective-permute-done((bf16[128,2048]{1,0:T(8,128)(2,1)S(1)}, bf16[128,2048]{1,0:T(8,128)(2,1)S(1)}, u32[]{:S(2)}, u32[]{:S(2)}) %collective-permute-start.12) | collective-permute-done | bytes 524320 | tf_op jit(solution)/shard_map/ppermute | solution.py:283
  47.1 0.9 %attend.1 = (bf16[2,256,512]{2,1,0:T(8,128)(2,1)S(1)}, bf16[2,256,512]{2,1,0:T(8,128)(2,1)S(1)}, bf16[2,8,256]{2,1,0:T(8,128)(2,1)S(1)}, f32[2,2,512]{2,1,0:T(2,128)S(1)}) custom-call(bf16[2,512]{1,0:T(2,128)(2,1)S(1)} %get-tuple-element.19.query, f32[8,128]{1,0:T(8,128)S(1)} %get-tuple-element.20.offset, f32[2,256,512]{2,1,0:T(8,128)S(1)} %project.3.refs_0_, ...), custom_call_target="tpu_custom_call" | custom-call | flops 1073741824 | tf_op jit(solution)/shard_map/attend/pallas_call | solution.py:367
  48.1 2.6 %collective-permute-start.18 = (f32[2,2,512]{2,1,0:T(2,128)S(1)}, f32[2,2,512]{2,1,0:T(2,128)S(1)}, u32[]{:S(2)}, u32[]{:S(2)}) collective-permute-start(f32[2,2,512]{2,1,0:T(2,128)S(1)} %get-tuple-element.33), channel_id=1, source_target_pairs={{0,22},{2,20},{4,18},{6,16},{8,30},{10,28},{12,26},{14,24},{16,6},... | collective-permute-start | bytes 24584 | tf_op jit(solution)/shard_map/ppermute | solution.py:397
  52.1 1.6 %collective-permute-done.19.refs_2_ = f32[2,2,512]{2,1,0:T(2,128)S(1)} collective-permute-done((f32[2,2,512]{2,1,0:T(2,128)S(1)}, f32[2,2,512]{2,1,0:T(2,128)S(1)}, u32[]{:S(2)}, u32[]{:S(2)}) %collective-permute-start.19) | collective-permute-done | bytes 8224 | tf_op jit(solution)/shard_map/ppermute | solution.py:397
  54.5 2.2 %collective-permute-start.22 = (f32[2,2,512]{2,1,0:T(2,128)S(1)}, f32[2,2,512]{2,1,0:T(2,128)S(1)}, u32[]{:S(2)}, u32[]{:S(2)}) collective-permute-start(f32[2,2,512]{2,1,0:T(2,128)S(1)} %combine.2), channel_id=1, source_target_pairs={{0,24},{2,26},{4,28},{6,30},{8,16},{10,18},{12,20},{14,22},{16,8},... | collective-permute-start | bytes 24584 | tf_op jit(solution)/shard_map/ppermute | solution.py:397
  56.7 1.0 %store.1 = (bf16[2,256,512]{2,1,0:T(8,128)(2,1)}, bf16[2,256,512]{2,1,0:T(8,128)(2,1)}, bf16[2,8,256]{2,1,0:T(8,128)(2,1)}) custom-call(bf16[2,256,512]{2,1,0:T(8,128)(2,1)S(1)} %get-tuple-element.27.keys, bf16[2,256,512]{2,1,0:T(8,128)(2,1)S(1)} %get-tuple-element.28.values, bf16[2,8,256]{2,1,0:T(8,128)(2,1)S(1)} %get-tuple-element.29.bias), custom_call_target="tpu_custom_call" | custom-call | tf_op jit(solution)/shard_map/store/pallas_call | solution.py:376
  58.5 0.8 %combine.3 = f32[2,512]{1,0:T(2,128)} custom-call(f32[2,2,512]{2,1,0:T(2,128)S(1)} %collective-permute-done.21.refs_0_, f32[2,2,512]{2,1,0:T(2,128)S(1)} %collective-permute-done.22.refs_1_), custom_call_target="tpu_custom_call" | custom-call | tf_op jit(solution)/shard_map/combine/pallas_call | solution.py:245
  (31 shorter events, 8.2 us)
Async XLA Ops:
  1.9 6.6 %collective-permute-start.1 = (bf16[256,512]{1,0:T(8,128)(2,1)S(1)}, bf16[256,512]{1,0:T(8,128)(2,1)S(1)}, u32[]{:S(2)}, u32[]{:S(2)}) collective-permute-start(bf16[256,512]{1,0:T(8,128)(2,1)S(1)} %get-tuple-element.23.refs_2_.refs_1_), channel_id=1, source_target_pairs={{0,20},{20,0},{4,24},{24,4},{8,28},{28,8},{12,30},{30,12},{14,26},... | collective-permute-start | bytes 786440 | tf_op jit(solution)/shard_map/ppermute | solution.py:286
  4.4 6.9 %collective-permute-start = (bf16[256,512]{1,0:T(8,128)(2,1)S(1)}, bf16[256,512]{1,0:T(8,128)(2,1)S(1)}, u32[]{:S(2)}, u32[]{:S(2)}) collective-permute-start(bf16[256,512]{1,0:T(8,128)(2,1)S(1)} %get-tuple-element.24.refs_9_.refs_8_), channel_id=1, source_target_pairs={{0,20},{20,0},{4,24},{24,4},{8,28},{28,8},{12,30},{30,12},{14,26},... | collective-permute-start | bytes 786440 | tf_op jit(solution)/shard_map/ppermute | solution.py:286
  8.5 6.4 %collective-permute-start.3 = (bf16[256,512]{1,0:T(8,128)(2,1)S(1)}, bf16[256,512]{1,0:T(8,128)(2,1)S(1)}, u32[]{:S(2)}, u32[]{:S(2)}) collective-permute-start(bf16[256,512]{1,0:T(8,128)(2,1)S(1)} %collective-permute-done.1.refs_10_.refs_9_), channel_id=1, source_target_pairs={{16,4},{4,16},{20,8},{8,20},{24,12},{12,24},{28,14},{14,28},{30,10... | collective-permute-start | bytes 786440 | tf_op jit(solution)/shard_map/ppermute | solution.py:286
  11.3 6.4 %collective-permute-start.4 = (bf16[256,512]{1,0:T(8,128)(2,1)S(1)}, bf16[256,512]{1,0:T(8,128)(2,1)S(1)}, u32[]{:S(2)}, u32[]{:S(2)}) collective-permute-start(bf16[256,512]{1,0:T(8,128)(2,1)S(1)} %collective-permute-done.refs_3_.refs_2_), channel_id=1, source_target_pairs={{16,4},{4,16},{20,8},{8,20},{24,12},{12,24},{28,14},{14,28},{30,10... | collective-permute-start | bytes 786440 | tf_op jit(solution)/shard_map/ppermute | solution.py:286
  13.3 6.3 %collective-permute-start.2 = (bf16[256,512]{1,0:T(8,128)(2,1)S(1)}, bf16[256,512]{1,0:T(8,128)(2,1)S(1)}, u32[]{:S(2)}, u32[]{:S(2)}) collective-permute-start(bf16[256,512]{1,0:T(8,128)(2,1)S(1)} %collective-permute-done.1.refs_10_.refs_9_), channel_id=1, source_target_pairs={{0,16},{16,0},{1,17},{17,1},{2,18},{18,2},{3,19},{19,3},{4,20},{20... | collective-permute-start | bytes 786440 | tf_op jit(solution)/shard_map/ppermute | solution.py:289
  13.7 7.5 %collective-permute-start.9 = (bf16[256,512]{1,0:T(8,128)(2,1)S(1)}, bf16[256,512]{1,0:T(8,128)(2,1)S(1)}, u32[]{:S(2)}, u32[]{:S(2)}) collective-permute-start(bf16[256,512]{1,0:T(8,128)(2,1)S(1)} %collective-permute-done.refs_3_.refs_2_), channel_id=1, source_target_pairs={{0,16},{16,0},{1,17},{17,1},{2,18},{18,2},{3,19},{19,3},{4,20},{20... | collective-permute-start | bytes 786440 | tf_op jit(solution)/shard_map/ppermute | solution.py:289
  14.9 7.9 %collective-permute-start.7 = (bf16[256,512]{1,0:T(8,128)(2,1)S(1)}, bf16[256,512]{1,0:T(8,128)(2,1)S(1)}, u32[]{:S(2)}, u32[]{:S(2)}) collective-permute-start(bf16[256,512]{1,0:T(8,128)(2,1)S(1)} %collective-permute-done.3.refs_5_.refs_4_), channel_id=1, source_target_pairs={{0,20},{20,0},{4,24},{24,4},{8,28},{28,8},{12,30},{30,12},{14,26},... | collective-permute-start | bytes 786440 | tf_op jit(solution)/shard_map/ppermute | solution.py:286
  17.7 6.4 %collective-permute-start.6 = (bf16[256,512]{1,0:T(8,128)(2,1)S(1)}, bf16[256,512]{1,0:T(8,128)(2,1)S(1)}, u32[]{:S(2)}, u32[]{:S(2)}) collective-permute-start(bf16[256,512]{1,0:T(8,128)(2,1)S(1)} %collective-permute-done.4.refs_12_.refs_11_), channel_id=1, source_target_pairs={{0,20},{20,0},{4,24},{24,4},{8,28},{28,8},{12,30},{30,12},{14,26},... | collective-permute-start | bytes 786440 | tf_op jit(solution)/shard_map/ppermute | solution.py:286
  19.6 5.7 %collective-permute-start.10 = (bf16[256,512]{1,0:T(8,128)(2,1)S(1)}, bf16[256,512]{1,0:T(8,128)(2,1)S(1)}, u32[]{:S(2)}, u32[]{:S(2)}) collective-permute-start(bf16[256,512]{1,0:T(8,128)(2,1)S(1)} %collective-permute-done.3.refs_5_.refs_4_), channel_id=1, source_target_pairs={{0,16},{16,0},{1,17},{17,1},{2,18},{18,2},{3,19},{19,3},{4,20},{20... | collective-permute-start | bytes 786440 | tf_op jit(solution)/shard_map/ppermute | solution.py:289
  19.6 6.3 %collective-permute-start.5 = (bf16[256,512]{1,0:T(8,128)(2,1)S(1)}, bf16[256,512]{1,0:T(8,128)(2,1)S(1)}, u32[]{:S(2)}, u32[]{:S(2)}) collective-permute-start(bf16[256,512]{1,0:T(8,128)(2,1)S(1)} %collective-permute-done.4.refs_12_.refs_11_), channel_id=1, source_target_pairs={{0,16},{16,0},{1,17},{17,1},{2,18},{18,2},{3,19},{19,3},{4,20},{20... | collective-permute-start | bytes 786440 | tf_op jit(solution)/shard_map/ppermute | solution.py:289
  21.2 14.9 %collective-permute-start.13 = (bf16[128,2048]{1,0:T(8,128)(2,1)S(1)}, bf16[128,2048]{1,0:T(8,128)(2,1)S(1)}, u32[]{:S(2)}, u32[]{:S(2)}) collective-permute-start(bf16[128,2048]{1,0:T(8,128)(2,1)S(1)} %get-tuple-element.22.refs_1_.refs_4_), channel_id=1, source_target_pairs={{1,0},{0,1},{3,2},{2,3},{5,4},{4,5},{7,6},{6,7},{9,8},{8,9},{11,10... | collective-permute-start | bytes 1572872 | tf_op jit(solution)/shard_map/ppermute | solution.py:283
  22.8 23.6 %collective-permute-start.12 = (bf16[128,2048]{1,0:T(8,128)(2,1)S(1)}, bf16[128,2048]{1,0:T(8,128)(2,1)S(1)}, u32[]{:S(2)}, u32[]{:S(2)}) collective-permute-start(bf16[128,2048]{1,0:T(8,128)(2,1)S(1)} %get-tuple-element.21.refs_0_.refs_3_), channel_id=1, source_target_pairs={{1,0},{0,1},{3,2},{2,3},{5,4},{4,5},{7,6},{6,7},{9,8},{8,9},{11,10... | collective-permute-start | bytes 1572872 | tf_op jit(solution)/shard_map/ppermute | solution.py:283
  24.1 2.3 %collective-permute-start.8 = (bf16[256,512]{1,0:T(8,128)(2,1)S(1)}, bf16[256,512]{1,0:T(8,128)(2,1)S(1)}, u32[]{:S(2)}, u32[]{:S(2)}) collective-permute-start(bf16[256,512]{1,0:T(8,128)(2,1)S(1)} %collective-permute-done.7.refs_14_.refs_13_), channel_id=1, source_target_pairs={{0,16},{16,0},{1,17},{17,1},{2,18},{18,2},{3,19},{19,3},{4,20},{20... | collective-permute-start | bytes 786440 | tf_op jit(solution)/shard_map/ppermute | solution.py:289
  25.2 5.8 %collective-permute-start.14 = (bf16[256,512]{1,0:T(8,128)(2,1)S(1)}, bf16[256,512]{1,0:T(8,128)(2,1)S(1)}, u32[]{:S(2)}, u32[]{:S(2)}) collective-permute-start(bf16[256,512]{1,0:T(8,128)(2,1)S(1)} %collective-permute-done.7.refs_14_.refs_13_), channel_id=1, source_target_pairs={{16,4},{4,16},{20,8},{8,20},{24,12},{12,24},{28,14},{14,28},{30,10... | collective-permute-start | bytes 786440 | tf_op jit(solution)/shard_map/ppermute | solution.py:286
  25.8 5.5 %collective-permute-start.11 = (bf16[256,512]{1,0:T(8,128)(2,1)S(1)}, bf16[256,512]{1,0:T(8,128)(2,1)S(1)}, u32[]{:S(2)}, u32[]{:S(2)}) collective-permute-start(bf16[256,512]{1,0:T(8,128)(2,1)S(1)} %collective-permute-done.6.refs_7_.refs_6_), channel_id=1, source_target_pairs={{0,16},{16,0},{1,17},{17,1},{2,18},{18,2},{3,19},{19,3},{4,20},{20... | collective-permute-start | bytes 786440 | tf_op jit(solution)/shard_map/ppermute | solution.py:289
  26.4 20.7 %collective-permute-start.16 = (bf16[2,8,128]{2,1,0:T(8,128)(2,1)S(1)}, bf16[2,8,128]{2,1,0:T(8,128)(2,1)S(1)}, u32[]{:S(2)}, u32[]{:S(2)}) collective-permute-start(bf16[2,8,128]{2,1,0:T(8,128)(2,1)S(1)} %get-tuple-element.26), channel_id=1, source_target_pairs={{1,0},{0,1},{3,2},{2,3},{5,4},{4,5},{7,6},{6,7},{9,8},{8,9},{11,10... | collective-permute-start | bytes 12296 | tf_op jit(solution)/shard_map/ppermute | solution.py:283
  31.0 16.0 %collective-permute-start.15 = (bf16[256,512]{1,0:T(8,128)(2,1)S(1)}, bf16[256,512]{1,0:T(8,128)(2,1)S(1)}, u32[]{:S(2)}, u32[]{:S(2)}) collective-permute-start(bf16[256,512]{1,0:T(8,128)(2,1)S(1)} %collective-permute-done.14.refs_7_), channel_id=1, source_target_pairs={{0,16},{16,0},{1,17},{17,1},{2,18},{18,2},{3,19},{19,3},{4,20},{20... | collective-permute-start | bytes 786440 | tf_op jit(solution)/shard_map/ppermute | solution.py:289
  48.0 3.4 %collective-permute-start.17 = (f32[2,2,512]{2,1,0:T(2,128)S(1)}, f32[2,2,512]{2,1,0:T(2,128)S(1)}, u32[]{:S(2)}, u32[]{:S(2)}) collective-permute-start(f32[2,2,512]{2,1,0:T(2,128)S(1)} %get-tuple-element.33), channel_id=1, source_target_pairs={{0,16},{2,18},{4,20},{6,22},{8,24},{10,26},{12,28},{14,30},{16,0},... | collective-permute-start | bytes 24584 | tf_op jit(solution)/shard_map/ppermute | solution.py:397
  48.1 4.0 %collective-permute-start.18 = (f32[2,2,512]{2,1,0:T(2,128)S(1)}, f32[2,2,512]{2,1,0:T(2,128)S(1)}, u32[]{:S(2)}, u32[]{:S(2)}) collective-permute-start(f32[2,2,512]{2,1,0:T(2,128)S(1)} %get-tuple-element.33), channel_id=1, source_target_pairs={{0,22},{2,20},{4,18},{6,16},{8,30},{10,28},{12,26},{14,24},{16,6},... | collective-permute-start | bytes 24584 | tf_op jit(solution)/shard_map/ppermute | solution.py:397
  50.6 3.1 %collective-permute-start.19 = (f32[2,2,512]{2,1,0:T(2,128)S(1)}, f32[2,2,512]{2,1,0:T(2,128)S(1)}, u32[]{:S(2)}, u32[]{:S(2)}) collective-permute-start(f32[2,2,512]{2,1,0:T(2,128)S(1)} %get-tuple-element.33), channel_id=1, source_target_pairs={{0,18},{2,16},{4,22},{6,20},{8,26},{10,24},{12,30},{14,28},{16,2},... | collective-permute-start | bytes 24584 | tf_op jit(solution)/shard_map/ppermute | solution.py:397
  50.9 3.1 %collective-permute-start.20 = (f32[2,2,512]{2,1,0:T(2,128)S(1)}, f32[2,2,512]{2,1,0:T(2,128)S(1)}, u32[]{:S(2)}, u32[]{:S(2)}) collective-permute-start(f32[2,2,512]{2,1,0:T(2,128)S(1)} %get-tuple-element.33), channel_id=1, source_target_pairs={{0,20},{2,22},{4,16},{6,18},{8,28},{10,30},{12,24},{14,26},{16,4},... | collective-permute-start | bytes 24584 | tf_op jit(solution)/shard_map/ppermute | solution.py:397
  54.0 3.7 %collective-permute-start.21 = (f32[2,2,512]{2,1,0:T(2,128)S(1)}, f32[2,2,512]{2,1,0:T(2,128)S(1)}, u32[]{:S(2)}, u32[]{:S(2)}) collective-permute-start(f32[2,2,512]{2,1,0:T(2,128)S(1)} %combine.2), channel_id=1, source_target_pairs={{0,16},{2,18},{4,20},{6,22},{8,24},{10,26},{12,28},{14,30},{16,0},... | collective-permute-start | bytes 24584 | tf_op jit(solution)/shard_map/ppermute | solution.py:397
  54.5 4.0 %collective-permute-start.22 = (f32[2,2,512]{2,1,0:T(2,128)S(1)}, f32[2,2,512]{2,1,0:T(2,128)S(1)}, u32[]{:S(2)}, u32[]{:S(2)}) collective-permute-start(f32[2,2,512]{2,1,0:T(2,128)S(1)} %combine.2), channel_id=1, source_target_pairs={{0,24},{2,26},{4,28},{6,30},{8,16},{10,18},{12,20},{14,22},{16,8},... | collective-permute-start | bytes 24584 | tf_op jit(solution)/shard_map/ppermute | solution.py:397
